TPU v7x, 256 devices: a whole 4x4x8 slice. The times are simulated.
256 devices in a mesh: ep: 64 (over z, x, core), tp: 4 (over y).
Axes of the slice: x: 4, y: 4, z: 8, core: 2. Of those that a mesh axis runs over, the one named last changes fastest.
Arguments:
- layer_in: bfloat16 [1024, 2048], P('ep'), may hold values from -6 to 6
- state_in: float32 [1024, 32, 4096], P('ep', 'tp'), may hold values from -6 to 6
- mix_gain: float32 [2048], replicated, may hold values from 0.1 to 1.9
- rec_weight: bfloat16 [2048, 2048], P('ep', 'tp'), may hold values from -0.125 to 0.125
- key_weight: bfloat16 [2048, 2048], P('ep', 'tp'), may hold values from -0.125 to 0.125
- val_weight: bfloat16 [2048, 2048], P('ep', 'tp'), may hold values from -0.125 to 0.125
- decay_down: bfloat16 [2048, 64], replicated, may hold values from -0.125 to 0.125
- decay_up: bfloat16 [64, 2048], P(None, 'tp'), may hold values from -0.75 to 0.75
- decay_base: float32 [2048], P('tp'), may hold values from -6 to 6
- rate_down: bfloat16 [2048, 64], replicated, may hold values from -0.125 to 0.125
- rate_up: bfloat16 [64, 2048], P(None, 'tp'), may hold values from -0.75 to 0.75
- rate_base: float32 [2048], P('tp'), may hold values from -6 to 6
- key_scale: float32 [2048], P('tp'), may hold values from 0.25 to 4
- group_gain: float32 [2048], P('tp'), may hold values from 0.1 to 1.9
- out_weight: bfloat16 [2048, 2048], P('tp', 'ep'), may hold values from -0.125 to 0.125
- post_gain: float32 [2048], replicated, may hold values from 0.1 to 1.9
- ffn_gain: float32 [2048], replicated, may hold values from 0.1 to 1.9
- routes: int32 [1024, 4], P('ep'), may hold values from 0 to 63, all different within a row; in each aligned block of 16 rows (0 to 15, 16 to 31, ...) at most 2 rows name the same one
- route_gates: float32 [1024, 4], P('ep'), may hold values from 0.05 to 1
- expert_gate: bfloat16 [64, 2048, 2048], P('ep', None, 'tp'), may hold values from -0.375 to 0.375
- expert_up: bfloat16 [64, 2048, 2048], P('ep', None, 'tp'), may hold values from -0.375 to 0.375
- expert_down: bfloat16 [64, 2048, 2048], P('ep', 'tp'), may hold values from -0.125 to 0.125
- out_gain: float32 [2048], replicated, may hold values from 0.1 to 1.9
Outputs:
- layer_out: bfloat16 [1024, 2048], P('ep')
- new_state: float32 [1024, 32, 4096], P('ep', 'tp')
Inputs may be any that keep to these rules, and one draw needn't show every extreme that they name: `routes`: each row names 4 different experts. Within the rows of one device (aligned blocks of 16 rows) no expert is named by more than 2 rows, and in every draw some block names some expert exactly 2 times.
All inputs are finite; a program needn't handle non-finite values.
Results may differ from a plain program's by a relative error of at most 0.017.
Values may be sent and summed in bfloat16 or wider, within the bound.
A program may use at most 128 MiB of HBM per device.

v0:
```python
import jax
import jax.numpy as jnp
from jax import lax
from jax.sharding import PartitionSpec as P

HEAD_DIM = 64


norm_eps = 1e-06
group_eps = 0.00064
clamp_limit = 7.0
gate_alpha = 1.702


def in_one_piece(arrays, axis, dim, along):
    both = jnp.concatenate(arrays, axis=along)
    result, at, gathered = (lax.all_gather(both, axis, axis=dim, tiled=True), 0, [])
    for a in arrays:
        gathered.append(lax.slice_in_dim(result, at, at + a.shape[along], axis=along))
        at += a.shape[along]
    return tuple(gathered)


def joined_along(tiles, dim):
    tiles = jnp.moveaxis(tiles, 0, dim)
    shape = tiles.shape
    return tiles.reshape(*shape[:dim], shape[dim] * shape[dim + 1], *shape[dim + 2 :])


def copy_for_each(shard, axis):
    copies = jnp.broadcast_to(shard, (lax.axis_size(axis), *shard.shape))
    return lax.all_to_all(copies, axis, split_axis=0, concat_axis=0, tiled=True)


def collect(shard, axis, dim):
    return joined_along(copy_for_each(shard, axis), dim)


def of_everyone(shard, axis):
    return copy_for_each(shard, axis).astype(jnp.float32).sum(axis=0)


def rms_scale(values, scales):
    return values * lax.rsqrt(jnp.mean(values * values, axis=-1, keepdims=True) + norm_eps) * scales


def rounded(values):
    return lax.optimization_barrier(values.astype(jnp.bfloat16)).astype(jnp.float32)


def local(
    layer_in,
    state_in,
    mix_gain,
    rec_weight,
    key_weight,
    val_weight,
    decay_down,
    decay_up,
    decay_base,
    rate_down,
    rate_up,
    rate_base,
    key_scale,
    group_gain,
    out_weight,
    post_gain,
    ffn_gain,
    routes,
    route_gates,
    expert_gate,
    expert_up,
    expert_down,
    out_gain,
):
    seq_count = layer_in.shape[0]
    model_width = layer_in.shape[1]
    head_count = state_in.shape[1]
    local_cols = rec_weight.shape[1]
    normed_in = rms_scale(layer_in.astype(jnp.float32), mix_gain).astype(jnp.bfloat16)
    pieces = in_one_piece((rec_weight, key_weight, val_weight), "ep", 0, 1)
    rec_sum, key_sum, val_sum = tuple(
        (
            jnp.dot(normed_in, weight_piece, preferred_element_type=jnp.float32)
            for weight_piece in pieces
        )
    )
    head_shape = (seq_count, head_count, HEAD_DIM)
    rec_rows = rounded(rec_sum).reshape(head_shape)
    key_rows = rounded(key_sum).reshape(head_shape)
    val_rows = rounded(val_sum).reshape(head_shape)
    decay_hidden = jnp.tanh(
        jnp.dot(normed_in, decay_down, preferred_element_type=jnp.float32)
    ).astype(jnp.bfloat16)
    rate_hidden = jnp.dot(normed_in, rate_down, preferred_element_type=jnp.float32).astype(
        jnp.bfloat16
    )
    decay_pre = decay_base + jnp.dot(decay_hidden, decay_up, preferred_element_type=jnp.float32)
    decay_factor = jnp.exp(-jnp.exp(-jax.nn.softplus(-decay_pre) - 0.5)).reshape(head_shape)
    learn_rate = jax.nn.sigmoid(
        rate_base + jnp.dot(rate_hidden, rate_up, preferred_element_type=jnp.float32)
    ).reshape(head_shape)
    scaled_key = key_rows * key_scale.reshape(head_count, HEAD_DIM)
    unit_key = scaled_key * lax.rsqrt(
        jnp.sum(scaled_key * scaled_key, axis=-1, keepdims=True) + norm_eps
    )
    old_state = state_in.reshape(seq_count, head_count, HEAD_DIM, HEAD_DIM)
    along_key = jnp.sum(old_state * unit_key[:, :, None, :], axis=-1)
    new_state = (
        old_state * decay_factor[:, :, None, :]
        - along_key[..., None] * (unit_key * learn_rate)[:, :, None, :]
        + val_rows[..., None] * (key_rows * learn_rate)[:, :, None, :]
    )
    readout = jnp.sum(new_state * rec_rows[:, :, None, :], axis=-1)
    centred = readout - jnp.mean(readout, axis=-1, keepdims=True)
    normed_out = centred * lax.rsqrt(
        jnp.mean(centred * centred, axis=-1, keepdims=True) + group_eps
    )
    normed_out = (
        (normed_out * group_gain.reshape(head_count, HEAD_DIM))
        .reshape(seq_count, local_cols)
        .astype(jnp.bfloat16)
    )
    head_partial = jnp.dot(
        normed_out, collect(out_weight, "ep", 1), preferred_element_type=jnp.float32
    )
    mix_sum = of_everyone(head_partial.astype(jnp.bfloat16), "tp").astype(jnp.float32)
    middle = (layer_in.astype(jnp.float32) + rms_scale(mix_sum, post_gain)).astype(jnp.bfloat16)
    ffn_in = rms_scale(middle.astype(jnp.float32), ffn_gain).astype(jnp.bfloat16)
    top_count = routes.shape[1]
    local_experts = expert_gate.shape[0]
    expert_total = lax.axis_size("ep") * local_experts
    capacity = max(2, 2 * seq_count * top_count // expert_total)
    slot_total = expert_total * capacity
    flat_routes = routes.reshape(-1)
    onehot = (flat_routes[:, None] == jnp.arange(expert_total, dtype=jnp.int32)[None, :]).astype(
        jnp.int32
    )
    slot_rank = jnp.sum((jnp.cumsum(onehot, axis=0) - 1) * onehot, axis=1)
    slot_index = flat_routes * capacity + slot_rank
    slot_range = jnp.arange(slot_total, dtype=jnp.int32)
    dispatch_table = jnp.sum(
        (slot_range[:, None] == slot_index[None, :])
        .astype(jnp.bfloat16)
        .reshape(slot_total, seq_count, top_count),
        axis=2,
    )
    send_rows = jnp.dot(dispatch_table, ffn_in, preferred_element_type=jnp.float32).astype(
        jnp.bfloat16
    )
    send_rows = send_rows.reshape(lax.axis_size("ep"), local_experts, capacity, model_width)
    arrived = lax.all_to_all(send_rows, "ep", split_axis=0, concat_axis=0, tiled=True)
    gate_cut = jnp.minimum(
        jnp.einsum("seid,edf->seif", arrived, expert_gate, preferred_element_type=jnp.float32),
        clamp_limit,
    )
    up_cut = jnp.clip(
        jnp.einsum("seid,edf->seif", arrived, expert_up, preferred_element_type=jnp.float32),
        -clamp_limit,
        clamp_limit,
    )
    hidden = ((up_cut + 1.0) * gate_cut * jax.nn.sigmoid(gate_alpha * gate_cut)).astype(
        jnp.bfloat16
    )
    partial_value = jnp.einsum(
        "seif,efd->seid", hidden, expert_down, preferred_element_type=jnp.float32
    )
    returned = (
        of_everyone(partial_value.astype(jnp.bfloat16), "tp")
        .astype(jnp.float32)
        .astype(jnp.bfloat16)
    )
    back_rows = lax.all_to_all(returned, "ep", split_axis=0, concat_axis=0, tiled=True)
    back_flat = back_rows.reshape(slot_total, model_width)
    combine_table = (slot_index[:, None] == slot_range[None, :]).astype(jnp.bfloat16)
    picked = jnp.dot(combine_table, back_flat, preferred_element_type=jnp.float32)
    moe_sum = jnp.sum(
        route_gates[:, :, None] * picked.reshape(seq_count, top_count, model_width), axis=1
    )
    layer_out = (middle.astype(jnp.float32) + rms_scale(moe_sum, out_gain)).astype(jnp.bfloat16)
    return (layer_out, new_state.reshape(seq_count, head_count, HEAD_DIM * HEAD_DIM))


def solution(mesh):
    in_specs = (
        P("ep", None),
        P("ep", "tp", None),
        P(),
        P("ep", "tp"),
        P("ep", "tp"),
        P("ep", "tp"),
        P(),
        P(None, "tp"),
        P("tp"),
        P(),
        P(None, "tp"),
        P("tp"),
        P("tp"),
        P("tp"),
        P("tp", "ep"),
        P(),
        P(),
        P("ep", None),
        P("ep", None),
        P("ep", None, "tp"),
        P("ep", None, "tp"),
        P("ep", "tp", None),
        P(),
    )
    out_specs = (P("ep", None), P("ep", "tp", None))
    return jax.shard_map(local, mesh=mesh, in_specs=in_specs, out_specs=out_specs, check_vma=False)
```

profile of v0, /device:TPU:1, one launch (start us, length us, event | category | flops | bytes accessed | tf_op | source)
XLA Modules:
  0.0 259.7 jit_solution(16564295580104135240)
XLA Ops:
  8.8 2.4 broadcast_in_dim.6
  11.3 13.3 %all-to-all-start = ((bf16[64,512,32]{1,2,0:T(8,128)(2,1)}), bf16[64,512,32]{1,2,0:T(8,128)(2,1)}, u32[]{:S(2)}, u32[]{:S(2)}) async-start(bf16[64,512,32]{1,2,0:T(8,128)(2,1)} %broadcast_in_dim.6), calls=%async_computation | async-start | bytes 4194304 | tf_op jit(solution)/shard_map/all_to_all | solution.py:32
  25.8 4.6 %reshape.253 = f32[16,8,64,64]{3,2,1,0:T(8,128)} reshape(f32[16,8,4096]{2,1,0:T(8,128)} %param.24) | data formatting | bytes 4194304 | tf_op jit(solution)/shard_map/reshape | solution.py:107
  30.5 2.3 mul.298
  32.8 4.8 %mul.322 = f32[16,8,4096]{2,1,0:T(8,128)} reshape(f32[16,8,64,64]{3,2,1,0:T(8,128)} %mul.298) | data formatting | bytes 4194304 | tf_op jit(solution)/shard_map/mul | solution.py:110
  38.4 62.9 %all-gather.2.cloned.1.call-done = bf16[2048,1536]{1,0:T(8,128)(2,1)} async-done(((bf16[32,1536]{1,0:T(8,128)(2,1)}), bf16[2048,1536]{1,0:T(8,128)(2,1)}) %all-gather.2.cloned.1.call-update) | async-done | bytes 6291472 | tf_op jit(solution)/shard_map/all_gather | solution.py:17
  101.4 2.0 fusion.43
  103.5 2.0 fusion.49
  105.6 2.0 fusion.46
  107.9 20.4 %broadcast_multiply_fusion = (f32[16,8,64,64]{3,2,1,0:T(8,128)}, f32[16,8,64]{2,1,0:T(8,128)S(1)}, f32[16,8,64,64]{3,2,1,0:T(8,128)}) fusion(f32[16,8,64]{2,1,0:T(8,128)S(1)} %get-tuple-element.10, f32[16,8,64]{2,1,0:T(8,128)S(1)} %reshape.267, f32[16,8,64]{2,1,0:T(8,128)S(1)} %reshape.268, f32[16,8,64,64]{3,2,1,0:T(8,128)} %reshape.253, ...), kind=kOutput, calls=%fused_computation.22 | output fusion | flops 4194367 | bytes 6520832 | tf_op jit(solution)/shard_map/mul | solution.py:111
  128.2 4.8 %mul.324 = f32[16,8,4096]{2,1,0:T(8,128)} reshape(f32[16,8,64,64]{3,2,1,0:T(8,128)} %get-tuple-element.11) | data formatting | bytes 4194304 | tf_op jit(solution)/shard_map/mul | solution.py:111
  133.0 4.8 %mul.325 = f32[16,8,4096]{2,1,0:T(8,128)} reshape(f32[16,8,64,64]{3,2,1,0:T(8,128)} %get-tuple-element.8) | data formatting | bytes 4194304 | tf_op jit(solution)/shard_map/mul | solution.py:112
  137.8 2.2 mul.320
  140.0 4.8 %mul.326 = f32[16,8,4096]{2,1,0:T(8,128)} reshape(f32[16,8,64,64]{3,2,1,0:T(8,128)} %mul.320) | data formatting | bytes 4194304 | tf_op jit(solution)/shard_map/mul | solution.py:114
  144.7 5.8 %multiply_reduce_fusion.2 = (f32[16,8]{1,0:T(8,128)S(1)}, f32[16,8,4096]{2,1,0:T(8,128)}) fusion(f32[16,8,4096]{2,1,0:T(8,128)} %mul.326, f32[16,8,4096]{2,1,0:T(8,128)} %mul.325, f32[16,8,4096]{2,1,0:T(8,128)} %mul.324, f32[16,8,4096]{2,1,0:T(8,128)} %param.24, f32[16,8,4096]{2,1,0:T(8,128)} %mul.322), kind=kLoop, calls=%fused_computation.20 | loop fusion | flops 2621312 | bytes 12583424 | tf_op jit(solution)/shard_map/reduce_sum | solution.py:115
  151.0 2.2 convolution_convert_fusion.2
  153.9 4.2 %all-to-all-start.1 = ((bf16[4,16,2048]{2,1,0:T(8,128)(2,1)}), bf16[4,16,2048]{2,1,0:T(8,128)(2,1)S(1)}, u32[]{:S(2)}, u32[]{:S(2)}) async-start(bf16[4,16,2048]{2,1,0:T(8,128)(2,1)} %broadcast_in_dim.7), calls=%async_computation.1 | async-start | bytes 524288 | tf_op jit(solution)/shard_map/all_to_all | solution.py:32
  158.2 5.8 %all-to-all-done.1 = bf16[4,16,2048]{2,1,0:T(8,128)(2,1)S(1)} async-done(((bf16[4,16,2048]{2,1,0:T(8,128)(2,1)}), bf16[4,16,2048]{2,1,0:T(8,128)(2,1)S(1)}, u32[]{:S(2)}, u32[]{:S(2)}) %all-to-all-start.1) | async-done | bytes 262176 | tf_op jit(solution)/shard_map/all_to_all | solution.py:32
  165.1 26.0 %all_to_all.25 = bf16[64,1,2,2048]{3,2,1,0:T(2,128)(2,1)S(1)} all-to-all(bf16[64,1,2,2048]{3,2,1,0:T(2,128)(2,1)S(1)} %bitcast.56), channel_id=1, replica_groups=mesh['ep'=64,'tp'=4] {'ep'}, dimensions={0} | all-to-all | bytes 1048576 | tf_op jit(solution)/shard_map/all_to_all | solution.py:152
  191.1 2.0 fusion.21
  193.2 2.5 convolution_convert_fusion
  195.9 29.3 %all_to_all.26 = bf16[4,64,1,2,2048]{4,1,3,2,0:T(8,128)(2,1)} all-to-all(bf16[4,64,1,2,2048]{4,1,3,2,0:T(8,128)(2,1)S(1)} %broadcast_in_dim.8), channel_id=1, replica_groups=mesh['ep'=64,'tp'=4] {'tp'}, dimensions={0} | all-to-all | bytes 4194304 | tf_op jit(solution)/shard_map/all_to_all | solution.py:32
  225.2 2.0 reduce_sum.148
  227.8 23.7 %all_to_all.27 = bf16[64,1,2,2048]{3,2,1,0:T(2,128)(2,1)S(1)} all-to-all(bf16[64,1,2,2048]{3,2,1,0:T(2,128)(2,1)S(1)} %copy.53), channel_id=1, replica_groups=mesh['ep'=64,'tp'=4] {'ep'}, dimensions={0} | all-to-all | bytes 1048576 | tf_op jit(solution)/shard_map/all_to_all | solution.py:173
  (79 shorter events, 8.5 us)
Async XLA Ops:
  7.2 186.0 %copy-start = (bf16[1,512,2048]{2,1,0:T(8,128)(2,1)S(1)}, bf16[1,512,2048]{2,1,0:T(8,128)(2,1)}, u32[]{:S(2)}) copy-start(bf16[1,512,2048]{2,1,0:T(8,128)(2,1)} %param.44) | copy-start | bytes 6291460
  7.2 94.2 %all-gather.2.cloned.1.call-start = ((), (), s32[]{:S(2)}) async-start(), calls=%async_computation.5 | async-start | bytes 6389760 | tf_op jit(solution)/shard_map/all_gather | solution.py:17
  11.2 13.4 %copy-start.1 = (bf16[16,2048]{1,0:T(8,128)(2,1)S(1)}, bf16[16,2048]{1,0:T(8,128)(2,1)}, u32[]{:S(2)}) copy-start(bf16[16,2048]{1,0:T(8,128)(2,1)} %param.23) | copy-start | bytes 196612
  11.2 13.5 %copy-start.11 = (f32[512]{0:T(512)S(1)}, f32[512]{0:T(512)}, u32[]{:S(2)}) copy-start(f32[512]{0:T(512)} %param.35) | copy-start | bytes 6148
  11.2 13.6 %copy-start.5 = (f32[2048]{0:T(1024)S(1)}, f32[2048]{0:T(1024)}, u32[]{:S(2)}) copy-start(f32[2048]{0:T(1024)} %param.25) | copy-start | bytes 24580
  11.2 13.6 %copy-start.13 = (bf16[2048,64]{0,1:T(8,128)(2,1)S(1)}, bf16[2048,64]{0,1:T(8,128)(2,1)}, u32[]{:S(2)}) copy-start(bf16[2048,64]{0,1:T(8,128)(2,1)} %param.32) | copy-start | bytes 786436
  11.2 13.6 %copy-start.14 = (bf16[64,512]{1,0:T(8,128)(2,1)S(1)}, bf16[64,512]{1,0:T(8,128)(2,1)}, u32[]{:S(2)}) copy-start(bf16[64,512]{1,0:T(8,128)(2,1)} %param.33) | copy-start | bytes 196612
  11.2 13.6 %copy-start.15 = (f32[512]{0:T(512)S(1)}, f32[512]{0:T(512)}, u32[]{:S(2)}) copy-start(f32[512]{0:T(512)} %param.34) | copy-start | bytes 6148
  11.2 14.1 %copy-start.2 = (bf16[2048,64]{0,1:T(8,128)(2,1)S(1)}, bf16[2048,64]{0,1:T(8,128)(2,1)}, u32[]{:S(2)}) copy-start(bf16[2048,64]{0,1:T(8,128)(2,1)} %param.29) | copy-start | bytes 786436
  11.2 14.1 %copy-start.3 = (bf16[64,512]{1,0:T(8,128)(2,1)S(1)}, bf16[64,512]{1,0:T(8,128)(2,1)}, u32[]{:S(2)}) copy-start(bf16[64,512]{1,0:T(8,128)(2,1)} %param.30) | copy-start | bytes 196612
  11.3 14.1 %copy-start.9 = (f32[512]{0:T(512)S(1)}, f32[512]{0:T(512)}, u32[]{:S(2)}) copy-start(f32[512]{0:T(512)} %param.31) | copy-start | bytes 6148
  11.3 139.7 %all-to-all-start = ((bf16[64,512,32]{1,2,0:T(8,128)(2,1)}), bf16[64,512,32]{1,2,0:T(8,128)(2,1)}, u32[]{:S(2)}, u32[]{:S(2)}) async-start(bf16[64,512,32]{1,2,0:T(8,128)(2,1)} %broadcast_in_dim.6), calls=%async_computation | async-start | bytes 4194304 | tf_op jit(solution)/shard_map/all_to_all | solution.py:32
  32.8 4.8 %copy-start.12 = (f32[512]{0:T(512)S(1)}, f32[512]{0:T(512)}, u32[]{:S(2)}) copy-start(f32[512]{0:T(512)} %param.36) | copy-start | bytes 6148
  32.8 4.9 %copy-start.8 = (s32[16,4]{0,1:T(4,128)S(1)}, s32[16,4]{0,1:T(4,128)}, u32[]{:S(2)}) copy-start(s32[16,4]{0,1:T(4,128)} %param.40) | copy-start | bytes 772
  150.6 13.7 %copy-start.6 = (f32[2048]{0:T(1024)S(1)}, f32[2048]{0:T(1024)}, u32[]{:S(2)}) copy-start(f32[2048]{0:T(1024)} %param.38) | copy-start | bytes 24580
  150.6 13.9 %copy-start.4 = (f32[2048]{0:T(1024)S(1)}, f32[2048]{0:T(1024)}, u32[]{:S(2)}) copy-start(f32[2048]{0:T(1024)} %param.39) | copy-start | bytes 24580
  153.9 10.1 %all-to-all-start.1 = ((bf16[4,16,2048]{2,1,0:T(8,128)(2,1)}), bf16[4,16,2048]{2,1,0:T(8,128)(2,1)S(1)}, u32[]{:S(2)}, u32[]{:S(2)}) async-start(bf16[4,16,2048]{2,1,0:T(8,128)(2,1)} %broadcast_in_dim.7), calls=%async_computation.1 | async-start | bytes 524288 | tf_op jit(solution)/shard_map/all_to_all | solution.py:32
  227.2 24.4 %copy-start.10 = (f32[16,4]{0,1:T(4,128)S(1)}, f32[16,4]{0,1:T(4,128)}, u32[]{:S(2)}) copy-start(f32[16,4]{0,1:T(4,128)} %param.41) | copy-start | bytes 772
  227.2 24.9 %copy-start.7 = (f32[2048]{0:T(1024)S(1)}, f32[2048]{0:T(1024)}, u32[]{:S(2)}) copy-start(f32[2048]{0:T(1024)} %param.45) | copy-start | bytes 24580
Sparse Core Ops, SparseCore 0:
  11.3 89.9 all-gather.1
where the time goes:
time: 261 us; the launch traced here: 260 us
  blocking collectives  78.9 us (30%)
  waiting for transfers between devices  68.8 us (26%)
  local copies, waits for them, and re-layouts  33.8 us (13%)
  other arithmetic  32.1 us (12%)
  starting transfers between devices  17.5 us (7%)
  between operations  14.3 us (5%)
  matrix products  14.2 us (5%)
    all_gather x1, waiting for transfers between devices, in_one_piece(): lax.all_gather(both, axis, axis=dim, tiled=True)  62.9 us
    all_to_all x1, blocking collectives, copy_for_each(): return lax.all_to_all(copies, axis, split_axis=0, concat_axis=0, tiled=True)  29.3 us
    all_to_all x1, blocking collectives, local(): lax.all_to_all(send_rows, 'ep', split_axis=0, concat_axis=0, tiled=True)  26 us
    all_to_all x1, blocking collectives, local(): lax.all_to_all(returned, 'ep', split_axis=0, concat_axis=0, tiled=True)  23.7 us
    mul x1, other arithmetic, local(): along_key[..., None] * (unit_key * learn_rate)[:, :, None, :]  20.4 us
    all_to_all x2, starting transfers between devices, copy_for_each(): return lax.all_to_all(copies, axis, split_axis=0, concat_axis=0, tiled=True)  17.5 us
    mul x3, local copies, waits for them, and re-layouts, local(): old_state * decay_factor[:, :, None, :]  7.23 us
    mul x3, local copies, waits for them, and re-layouts, local(): readout = jnp.sum(new_state * rec_rows[:, :, None, :], axis=-1)  7.04 us
  transfers between devices with their start and end apart: 3, of which 2 were waited for; matrix products, arithmetic and copies ran while one was open for 25% of the time, Pallas kernels for 0%

commit v1 on v0

v1 whole, which is shorter than its diff:
```python
import functools

import jax
import jax.numpy as jnp
from jax import lax
from jax.experimental import pallas as pl
from jax.experimental.pallas import tpu as pltpu
from jax.sharding import PartitionSpec as P

MESH = pl.DeviceIdType.MESH
HEAD_DIM = 64
CAP = 2
LANES = 128
WIDE = 256

norm_eps = 1e-06
group_eps = 0.00064
clamp_limit = 7.0
gate_alpha = 1.702

F32 = jnp.float32
BF16 = jnp.bfloat16


def dot(a, b):
    return lax.dot_general(a, b, (((1,), (0,)), ((), ())), preferred_element_type=F32)


def dot_t(a, b):
    return lax.dot_general(a, b, (((1,), (1,)), ((), ())), preferred_element_type=F32)


def split(a):
    high = a.astype(BF16)
    return high, (a - high.astype(F32)).astype(BF16)


def dot_split(a, b):
    high, low = split(a)
    return dot(high, b) + dot(low, b)


def iota(shape, dim):
    return lax.broadcasted_iota(jnp.int32, shape, dim)


def one_hot(mask):
    return jnp.where(mask, 1.0, 0.0).astype(BF16)


def rms_scale(values, scales):
    return values * lax.rsqrt(jnp.mean(values * values, axis=-1, keepdims=True) + norm_eps) * scales


def kernel(
    n_ep,
    n_tp,
    layer_in,
    state_in,
    mix_gain,
    rec_weight,
    key_weight,
    val_weight,
    decay_down,
    decay_up,
    decay_base,
    rate_down,
    rate_up,
    rate_base,
    key_scale,
    group_gain,
    out_weight,
    post_gain,
    ffn_gain,
    routes_t,
    routes,
    gates,
    expert_gate,
    expert_up,
    expert_down,
    out_gain,
    layer_out,
    new_state,
    state,
    w_gate,
    w_up,
    w_down,
    proj_send,
    proj_all,
    out_send,
    out_all,
    rows_all,
    normed_all,
    qkv_send,
    qkv_all,
    decay_rows,
    rate_rows,
    read_send,
    read_all,
    part_send,
    part_all,
    mix_rows,
    wide_rows,
    slot_send,
    slot_here,
    slot_all,
    down_send,
    down_all,
    back_send,
    back_all,
    moe_send,
    moe_all,
    load_sem,
    send_sem,
    recv_sem,
    slot_sem,
):
    seqs, width = layer_in.shape
    heads = state_in.shape[1]
    plane = heads
    n_z = n_ep // plane
    low = decay_down.shape[1]
    quarter = width // n_tp
    tiles = quarter // LANES
    slab = CAP * tiles
    rows = seqs * heads
    depth = rec_weight.shape[0]
    out_cols = out_weight.shape[1]

    me = lax.axis_index("ep")
    mine = lax.axis_index("tp")
    member = lax.rem(me, plane)
    base = me - member

    def ep_at(step):
        return lax.rem(me + step, n_ep)

    def member_at(step):
        return lax.rem(member + step, plane)

    def z_at(step):
        return lax.rem(me + step * plane, n_ep)

    def tp_at(step):
        return lax.rem(mine + step, n_tp)

    def send(src, dst, phase, ep, tp, sem=None):
        pltpu.make_async_remote_copy(
            src_ref=src,
            dst_ref=dst,
            send_sem=send_sem.at[phase],
            recv_sem=recv_sem.at[phase] if sem is None else sem,
            device_id={"ep": ep, "tp": tp},
            device_id_type=MESH,
        ).start()

    def keep(src, dst, sem):
        pltpu.make_async_copy(src, dst, sem).start()

    def arrive(buffer, sem):
        pltpu.make_async_copy(buffer, buffer, sem).wait()

    def sent(buffer, phase):
        pltpu.make_async_copy(buffer, buffer, send_sem.at[phase]).wait()

    def loop(start, stop, body):
        def step(i, carry):
            body(i)
            return carry

        lax.fori_loop(start, stop, step, 0)

    barrier = pltpu.get_barrier_semaphore()

    def greet(i):
        pl.semaphore_signal(barrier, inc=1, device_id={"ep": ep_at(i), "tp": mine}, device_id_type=MESH)

    loop(1, n_ep, greet)

    def greet_plane(i):
        pl.semaphore_signal(
            barrier,
            inc=1,
            device_id={"ep": base + member_at(lax.rem(i, plane)), "tp": tp_at(i // plane)},
            device_id_type=MESH,
        )

    loop(plane, plane * n_tp, greet_plane)

    loads = (
        (state_in, state),
        (expert_gate.at[0], w_gate),
        (expert_up.at[0], w_up),
        (expert_down.at[0], w_down),
    )
    for n, (src, dst) in enumerate(loads):
        pltpu.make_async_copy(src, dst, load_sem.at[n]).start()

    for h in range(heads):
        cut = slice(h * HEAD_DIM, (h + 1) * HEAD_DIM)
        proj_send[h, :depth, :] = jnp.concatenate([rec_weight[:, cut], key_weight[:, cut]], axis=1)
        proj_send[h, depth:, :] = jnp.concatenate(
            [val_weight[: depth // 2, cut], val_weight[depth // 2 :, cut]], axis=1
        )
    eye = one_hot(iota((out_cols, out_cols), 0) == iota((out_cols, out_cols), 1))
    out_send[...] = dot_t(eye, out_weight[...]).astype(BF16)

    pl.semaphore_wait(barrier, n_ep - 1 + plane * (n_tp - 1))

    keep(layer_in, rows_all.at[member], recv_sem.at[0])

    def send_rows(i):
        send(layer_in, rows_all.at[member], 0, base + member_at(i), mine)

    loop(1, plane, send_rows)
    keep(proj_send.at[member], proj_all.at[me], recv_sem.at[1])

    def send_proj(i):
        to = ep_at(i)
        send(proj_send.at[lax.rem(to, plane)], proj_all.at[me], 1, to, mine)

    loop(1, n_ep, send_proj)
    z_me = me // plane
    keep(out_send, out_all.at[z_me], recv_sem.at[2])

    def send_out(i):
        send(out_send, out_all.at[z_me], 2, z_at(i), mine)

    loop(1, n_z, send_out)

    own_normed = rms_scale(layer_in[...].astype(F32), mix_gain[...]).astype(BF16)
    decay_hidden = jnp.tanh(dot(own_normed, decay_down[...])).astype(BF16)
    rate_hidden = dot(own_normed, rate_down[...]).astype(BF16)
    decay_sig = jax.nn.sigmoid(decay_base[...] + dot(decay_hidden, decay_up[...]))
    decay = jnp.exp(-jnp.exp(jnp.full((), -0.5, F32)) * decay_sig)
    rate = jax.nn.sigmoid(rate_base[...] + dot(rate_hidden, rate_up[...]))
    for h in range(heads):
        cut = slice(h * HEAD_DIM, (h + 1) * HEAD_DIM)
        decay_rows[h * seqs : (h + 1) * seqs, :] = decay[:, cut]
        rate_rows[h * seqs : (h + 1) * seqs, :] = rate[:, cut]

    top = routes.shape[1]
    named_t = jnp.zeros((n_ep, seqs), F32)
    for j in range(top):
        named_t += jnp.where(iota((n_ep, seqs), 0) == routes_t[j : j + 1, :], 1.0, 0.0)
    before_t = dot(named_t.astype(BF16), one_hot(iota((seqs, seqs), 0) < iota((seqs, seqs), 1)))
    named = jnp.zeros((seqs, n_ep), F32)
    weight = jnp.zeros((seqs, n_ep), F32)
    for j in range(top):
        hit = iota((seqs, n_ep), 1) == routes[:, j : j + 1]
        named += jnp.where(hit, 1.0, 0.0)
        weight += jnp.where(hit, gates[:, j : j + 1], 0.0)
    before = dot(one_hot(iota((seqs, seqs), 1) < iota((seqs, seqs), 0)), named.astype(BF16))

    arrive(rows_all, recv_sem.at[0])

    def norm_rows(i):
        values = rms_scale(rows_all[i].astype(F32), mix_gain[...]).astype(BF16)
        normed_all[pl.ds(pl.multiple_of(i * seqs, seqs), seqs), :] = values

    loop(0, plane, norm_rows)

    arrive(proj_all, recv_sem.at[1])
    pairs = proj_all[:, :depth, :].reshape(n_ep * depth, 2 * HEAD_DIM)
    vals = proj_all[:, depth:, :]
    vals = jnp.concatenate([vals, vals], axis=1).reshape(n_ep * depth, 2 * HEAD_DIM)
    spread = (n_ep * depth, 2 * HEAD_DIM)
    first = lax.rem(iota(spread, 0), depth) < depth // 2
    vals = jnp.where(first == (iota(spread, 1) < HEAD_DIM), vals.astype(F32), 0.0).astype(BF16)
    normed = normed_all[...]
    pair_sum = dot(normed, pairs)
    val_sum = dot(normed, vals)
    val_sum = val_sum[:, :HEAD_DIM] + val_sum[:, HEAD_DIM:]
    together = jnp.concatenate([pair_sum, val_sum, jnp.zeros_like(val_sum)], axis=1)
    qkv_send[...] = together.astype(BF16).reshape(plane, seqs, WIDE)
    keep(qkv_send.at[member], qkv_all.at[member], recv_sem.at[3])

    def send_qkv(i):
        to = member_at(i)
        send(qkv_send.at[to], qkv_all.at[member], 3, base + to, mine)

    loop(1, plane, send_qkv)

    turn = one_hot(
        iota((rows, rows), 1)
        == lax.rem(iota((rows, rows), 0), heads) * seqs + iota((rows, rows), 0) // heads
    )
    turn_back = one_hot(
        iota((rows, rows), 1)
        == lax.rem(iota((rows, rows), 0), seqs) * heads + iota((rows, rows), 0) // seqs
    )
    decay_high, decay_low = split(decay_rows[...])
    rate_high, rate_low = split(rate_rows[...])
    turned = dot(turn, jnp.concatenate([decay_high, decay_low, rate_high, rate_low], axis=1))
    decay = turned[:, :HEAD_DIM] + turned[:, HEAD_DIM : 2 * HEAD_DIM]
    rate = turned[:, 2 * HEAD_DIM : 3 * HEAD_DIM] + turned[:, 3 * HEAD_DIM :]
    joined = one_hot(iota((WIDE, WIDE), 0) // HEAD_DIM == iota((WIDE, WIDE), 1) // HEAD_DIM)

    arrive(qkv_all, recv_sem.at[3])
    qkv = dot(turn, qkv_all[...].reshape(rows, WIDE))
    rec = qkv[:, :HEAD_DIM]
    key = qkv[:, HEAD_DIM : 2 * HEAD_DIM]
    val = qkv[:, 2 * HEAD_DIM : 3 * HEAD_DIM].astype(BF16)

    def of_heads(scales):
        return jnp.broadcast_to(scales[...][None], (seqs, heads, HEAD_DIM)).reshape(rows, HEAD_DIM)

    scaled = key * of_heads(key_scale)
    unit = scaled * lax.rsqrt(jnp.sum(scaled * scaled, axis=-1, keepdims=True) + norm_eps)

    def wide(a):
        return jnp.concatenate([a] * (WIDE // HEAD_DIM), axis=1)

    unit_w, decay_w, rec_w = wide(unit), wide(decay), wide(rec)
    unit_rate, key_rate = wide(unit * rate), wide(key * rate)
    per = WIDE // HEAD_DIM
    pltpu.make_async_copy(state_in, state, load_sem.at[0]).wait()

    def update(i, readout):
        lanes = pl.ds(pl.multiple_of(i * WIDE, WIDE), WIDE)
        old = state[:, :, lanes].reshape(rows, WIDE)
        along = dot_split(old * unit_w, joined)
        pick = one_hot(iota((HEAD_DIM, WIDE), 0) == i * per + iota((HEAD_DIM, WIDE), 1) // HEAD_DIM)
        gather = one_hot(iota((WIDE, HEAD_DIM), 1) == i * per + iota((WIDE, HEAD_DIM), 0) // HEAD_DIM)
        new = old * decay_w - along * unit_rate + dot(val, pick) * key_rate
        state[:, :, lanes] = new.reshape(seqs, heads, WIDE)
        return readout + dot_split(new * rec_w, gather)

    readout = lax.fori_loop(0, HEAD_DIM // per, update, jnp.zeros((rows, HEAD_DIM), F32))
    centred = readout - jnp.mean(readout, axis=-1, keepdims=True)
    normed_out = centred * lax.rsqrt(jnp.mean(centred * centred, axis=-1, keepdims=True) + group_eps)
    normed_out = dot(turn_back, (normed_out * of_heads(group_gain)).astype(BF16)).astype(BF16)
    for h in range(heads):
        read_send[:, h * HEAD_DIM : (h + 1) * HEAD_DIM] = normed_out[h * seqs : (h + 1) * seqs, :]
    keep(read_send, read_all.at[member], recv_sem.at[4])

    def send_read(i):
        send(read_send, read_all.at[member], 4, base + member_at(i), mine)

    loop(1, plane, send_read)
    pltpu.make_async_copy(state, new_state, load_sem.at[0]).start()

    arrive(out_all, recv_sem.at[2])
    arrive(read_all, recv_sem.at[4])
    part = dot_t(
        read_all[...].reshape(plane * seqs, quarter), out_all[...].reshape(n_z * out_cols, quarter)
    )
    part_send[...] = part.astype(BF16).reshape(plane, seqs, n_z * out_cols)
    keep(part_send.at[member], part_all.at[mine * plane + member], recv_sem.at[5])

    def send_part(i):
        to = member_at(lax.rem(i, plane))
        send(part_send.at[to], part_all.at[mine * plane + member], 5, base + to, tp_at(i // plane))

    loop(1, plane * n_tp, send_part)

    arrive(part_all, recv_sem.at[5])
    for g in range(plane):
        total = part_all[g].astype(F32)
        for t in range(1, n_tp):
            total += part_all[t * plane + g].astype(F32)
        for z in range(n_z):
            at = (z * plane + g) * out_cols
            mix_rows[:, at : at + out_cols] = total[:, z * out_cols : (z + 1) * out_cols]
    middle = (layer_in[...].astype(F32) + rms_scale(mix_rows[...], post_gain[...])).astype(BF16)
    mix_rows[...] = middle.astype(F32)
    ffn_in = rms_scale(mix_rows[...], ffn_gain[...])

    mix_rows[...] = ffn_in
    columns = pl.ds(pl.multiple_of(mine * quarter, quarter), quarter)
    ffn_cut = mix_rows[:, columns].astype(BF16)
    for s in range(CAP):
        chosen = jnp.where(before_t == float(s), named_t, 0.0).astype(BF16)
        values = dot(chosen, ffn_cut)
        for t in range(tiles):
            wide_rows[pl.ds(s * tiles + t, n_ep, stride=slab), :] = values[:, t * LANES : (t + 1) * LANES]
    slot_send[...] = wide_rows[...].astype(BF16).reshape(n_ep, slab, LANES)
    keep(slot_send.at[me], slot_here.at[me], recv_sem.at[6])

    def send_slot(i):
        to = ep_at(i)
        send(slot_send.at[to], slot_here.at[me], 6, to, mine)

    loop(1, n_ep, send_slot)
    mix_rows[...] = middle.astype(F32)

    arrive(slot_here, recv_sem.at[6])
    for step in range(1, n_tp):
        send(slot_here, slot_all.at[mine], 7, me, tp_at(step), slot_sem.at[mine])

    pltpu.make_async_copy(expert_gate.at[0], w_gate, load_sem.at[1]).wait()
    pltpu.make_async_copy(expert_up.at[0], w_up, load_sem.at[2]).wait()
    slots = CAP * n_ep

    def from_slabs(source):
        wide_rows[...] = source.astype(F32).reshape(n_ep * slab, LANES)
        return [
            [wide_rows[pl.ds(s * tiles + t, n_ep, stride=slab), :] for t in range(tiles)]
            for s in range(CAP)
        ]

    gate = up = None
    order = [0, 1, n_tp - 1] + list(range(2, n_tp - 1))
    for step in order[:n_tp]:
        at = tp_at(step)
        if step == 0:
            source = slot_here[...]
        else:
            arrive(slot_all.at[at], slot_sem.at[at])
            source = slot_all[at]
        part = jnp.concatenate([jnp.concatenate(p, axis=1) for p in from_slabs(source)], axis=0).astype(BF16)
        feats = pl.ds(pl.multiple_of(at * quarter, quarter), quarter)
        gate_part, up_part = dot(part, w_gate[feats, :]), dot(part, w_up[feats, :])
        gate = gate_part if gate is None else gate + gate_part
        up = up_part if up is None else up + up_part
    gate = jnp.minimum(gate, clamp_limit)
    up = jnp.clip(up, -clamp_limit, clamp_limit)
    hidden = ((up + 1.0) * gate * jax.nn.sigmoid(gate_alpha * gate)).astype(BF16)

    pltpu.make_async_copy(expert_down.at[0], w_down, load_sem.at[3]).wait()
    for step in list(range(1, n_tp)) + [0]:
        at = tp_at(step)
        feats = pl.ds(pl.multiple_of(at * quarter, quarter), quarter)
        values = dot(hidden, w_down[:, feats]).astype(BF16)
        if step == 0:
            down_all[mine] = values
        else:
            down_send[at] = values
            send(down_send.at[at], down_all.at[mine], 8, me, at, slot_sem.at[n_tp + mine])
    for step in range(1, n_tp):
        at = tp_at(step)
        arrive(down_all.at[at], slot_sem.at[n_tp + at])
    total = down_all[0].astype(F32)
    for t in range(1, n_tp):
        total += down_all[t].astype(F32)
    for s in range(CAP):
        for t in range(tiles):
            wide_rows[pl.ds(s * tiles + t, n_ep, stride=slab), :] = total[
                s * n_ep : (s + 1) * n_ep, t * LANES : (t + 1) * LANES
            ]
    back_send[...] = wide_rows[...].astype(BF16).reshape(n_ep, slab, LANES)
    keep(back_send.at[me], back_all.at[me], recv_sem.at[9])

    def send_back(i):
        to = ep_at(i)
        send(back_send.at[to], back_all.at[me], 9, to, mine)

    loop(1, n_ep, send_back)

    arrive(back_all, recv_sem.at[9])
    moe = jnp.zeros((seqs, quarter), F32)
    for s, p in enumerate(from_slabs(back_all[...])):
        moe += dot_split(jnp.where(before == float(s), weight, 0.0), jnp.concatenate(p, axis=1).astype(BF16))
    moe_send[...] = moe
    keep(moe_send, moe_all.at[mine], recv_sem.at[10])
    for step in range(1, n_tp):
        send(moe_send, moe_all.at[mine], 10, me, tp_at(step))
    arrive(moe_all, recv_sem.at[10])
    moe = jnp.concatenate([moe_all[t] for t in range(n_tp)], axis=1)
    layer_out[...] = (mix_rows[...] + rms_scale(moe, out_gain[...])).astype(BF16)

    pltpu.make_async_copy(state, new_state, load_sem.at[0]).wait()
    sent(rows_all.at[pl.ds(0, plane - 1)], 0)
    sent(proj_all.at[pl.ds(0, n_ep - 1)], 1)
    sent(out_all.at[pl.ds(0, n_z - 1)], 2)
    sent(qkv_all.at[pl.ds(0, plane - 1)], 3)
    sent(read_all.at[pl.ds(0, plane - 1)], 4)
    sent(part_all.at[pl.ds(0, n_tp * plane - 1)], 5)
    sent(slot_here.at[pl.ds(0, n_ep - 1)], 6)
    sent(slot_all.at[pl.ds(0, n_tp - 1)], 7)
    sent(down_all.at[pl.ds(0, n_tp - 1)], 8)
    sent(back_all.at[pl.ds(0, n_ep - 1)], 9)
    sent(moe_all.at[pl.ds(0, n_tp - 1)], 10)


def local(n_ep, n_tp, *args):
    (
        layer_in,
        state_in,
        mix_gain,
        rec_weight,
        key_weight,
        val_weight,
        decay_down,
        decay_up,
        decay_base,
        rate_down,
        rate_up,
        rate_base,
        key_scale,
        group_gain,
        out_weight,
        post_gain,
        ffn_gain,
        routes,
        route_gates,
        expert_gate,
        expert_up,
        expert_down,
        out_gain,
    ) = args
    seqs, width = layer_in.shape
    heads = state_in.shape[1]
    plane = heads
    n_z = n_ep // plane
    quarter = width // n_tp
    slab = CAP * (quarter // LANES)
    depth = rec_weight.shape[0]
    out_cols = out_weight.shape[1]
    hidden = expert_gate.shape[2]
    slots = CAP * n_ep
    state_lanes = state_in.shape[2]
    row = lambda a: a.reshape(1, -1)
    by_head = lambda a: a.reshape(heads, HEAD_DIM)
    operands = (
        layer_in,
        state_in,
        row(mix_gain),
        rec_weight,
        key_weight,
        val_weight,
        decay_down,
        decay_up,
        row(decay_base),
        rate_down,
        rate_up,
        row(rate_base),
        by_head(key_scale),
        by_head(group_gain),
        out_weight,
        row(post_gain),
        row(ffn_gain),
        routes.T,
        routes,
        route_gates,
        expert_gate,
        expert_up,
        expert_down,
        row(out_gain),
    )
    far = {1, 20, 21, 22}
    vmem = pl.BlockSpec(memory_space=pltpu.VMEM)
    hbm = pl.BlockSpec(memory_space=pl.ANY)
    scratch = [
        pltpu.VMEM(state_in.shape, F32),
        pltpu.VMEM((width, hidden), BF16),
        pltpu.VMEM((width, hidden), BF16),
        pltpu.VMEM((hidden, width), BF16),
        pltpu.VMEM((plane, depth + depth // 2, 2 * HEAD_DIM), BF16),
        pltpu.VMEM((n_ep, depth + depth // 2, 2 * HEAD_DIM), BF16),
        pltpu.VMEM((out_cols, quarter), BF16),
        pltpu.VMEM((n_z, out_cols, quarter), BF16),
        pltpu.VMEM((plane, seqs, width), BF16),
        pltpu.VMEM((plane * seqs, width), BF16),
        pltpu.VMEM((plane, seqs, WIDE), BF16),
        pltpu.VMEM((plane, seqs, WIDE), BF16),
        pltpu.VMEM((heads * seqs, HEAD_DIM), F32),
        pltpu.VMEM((heads * seqs, HEAD_DIM), F32),
        pltpu.VMEM((seqs, quarter), BF16),
        pltpu.VMEM((plane, seqs, quarter), BF16),
        pltpu.VMEM((plane, seqs, n_z * out_cols), BF16),
        pltpu.VMEM((n_tp * plane, seqs, n_z * out_cols), BF16),
        pltpu.VMEM((seqs, width), F32),
        pltpu.VMEM((n_ep * slab, LANES), F32),
        pltpu.VMEM((n_ep, slab, LANES), BF16),
        pltpu.VMEM((n_ep, slab, LANES), BF16),
        pltpu.VMEM((n_tp, n_ep, slab, LANES), BF16),
        pltpu.VMEM((n_tp, slots, quarter), BF16),
        pltpu.VMEM((n_tp, slots, quarter), BF16),
        pltpu.VMEM((n_ep, slab, LANES), BF16),
        pltpu.VMEM((n_ep, slab, LANES), BF16),
        pltpu.VMEM((seqs, quarter), F32),
        pltpu.VMEM((n_tp, seqs, quarter), F32),
        pltpu.SemaphoreType.DMA((4,)),
        pltpu.SemaphoreType.DMA((11,)),
        pltpu.SemaphoreType.DMA((11,)),
        pltpu.SemaphoreType.DMA((2 * n_tp,)),
    ]
    return pl.pallas_call(
        functools.partial(kernel, n_ep, n_tp),
        out_shape=(
            jax.ShapeDtypeStruct(layer_in.shape, BF16),
            jax.ShapeDtypeStruct((seqs, heads, state_lanes), F32),
        ),
        in_specs=[hbm if n in far else vmem for n in range(len(operands))],
        out_specs=(vmem, hbm),
        scratch_shapes=scratch,
        compiler_params=pltpu.CompilerParams(
            collective_id=0, has_side_effects=True, vmem_limit_bytes=48 * 1024 * 1024
        ),
    )(*operands)


def solution(mesh):
    in_specs = (
        P("ep", None),
        P("ep", "tp", None),
        P(),
        P("ep", "tp"),
        P("ep", "tp"),
        P("ep", "tp"),
        P(),
        P(None, "tp"),
        P("tp"),
        P(),
        P(None, "tp"),
        P("tp"),
        P("tp"),
        P("tp"),
        P("tp", "ep"),
        P(),
        P(),
        P("ep", None),
        P("ep", None),
        P("ep", None, "tp"),
        P("ep", None, "tp"),
        P("ep", "tp", None),
        P(),
    )
    out_specs = (P("ep", None), P("ep", "tp", None))
    body = functools.partial(local, mesh.shape["ep"], mesh.shape["tp"])
    return jax.shard_map(body, mesh=mesh, in_specs=in_specs, out_specs=out_specs, check_vma=False)
```

time: 261 us -> 114 us (0.44)
  Pallas kernels: 0 us -> 92.6 us
  blocking collectives: 78.9 us -> 0 us
  waiting for transfers between devices: 68.8 us -> 0 us
  other arithmetic: 32.1 us -> 0 us
  starting transfers between devices: 17.5 us -> 0 us
  local copies, waits for them, and re-layouts: 33.8 us -> 19.5 us
  matrix products: 14.2 us -> 0 us
  between operations: 14.3 us -> 0.68 us
    pallas_call x0 -> x1, Pallas kernels: none -> 92.6 us  [local(): pl.pallas_call(functools.partial(kernel, n_ep, n_tp), out_shape=(jax.Shap...]
    all_to_all x3 -> x0, blocking collectives: 78.9 us -> none  [the longest x1 29.3 us: copy_for_each(): return lax.all_to_all(copies, axis, split_axis=0, concat_axis=0, tiled=True)]
    all_gather x1 -> x0, waiting for transfers between devices: 62.9 us -> none  [in_one_piece(): lax.all_gather(both, axis, axis=dim, tiled=True)]
    mul x11 -> x0, local copies, waits for them, and re-layouts: 24.1 us -> none  [the longest x3 7.23 us: local(): old_state * decay_factor[:, :, None, :]]
    mul x2 -> x0, other arithmetic: 20.4 us -> none  [the longest x1 20.4 us: local(): along_key[..., None] * (unit_key * learn_rate)[:, :, None, :]]
    unnamed x33 -> x35, local copies, waits for them, and re-layouts: 0.17 us -> 18 us
    all_to_all x2 -> x0, starting transfers between devices: 17.5 us -> none  [copy_for_each(): return lax.all_to_all(copies, axis, split_axis=0, concat_axis=0, tiled=True)]
    dot_general x10 -> x0, matrix products: 14.2 us -> none  [the longest x3 6.04 us: local(): jnp.dot(normed_in, weight_piece, preferred_element_type=jnp.float32)]
  transfers between devices with their start and end apart: 3 -> 0, of which waited for: 2 -> 0; matrix products, arithmetic and copies ran while one was open for 25% -> 0% of each run, Pallas kernels for 0% -> 0%
where the time goes in v1:
time: 114 us; the launch traced here: 113 us
  Pallas kernels  92.6 us (81%)
  local copies, waits for them, and re-layouts  19.5 us (17%)
    pallas_call x1, Pallas kernels, local(): pl.pallas_call(functools.partial(kernel, n_ep, n_tp), out_shape=(jax.Shap...  92.6 us
    unnamed x35, local copies, waits for them, and re-layouts  18 us

profile of v1, /device:TPU:1, one launch (start us, length us, event | category | flops | bytes accessed | tf_op | source)
XLA Modules:
  0.0 112.8 jit_solution(14275238785768957266)
XLA Ops:
  0.6 0.8 reshape.31.key_scale
  1.4 0.8 reshape.32.group_gain
  2.1 0.8 copy.29.gates
  2.9 0.8 copy.28.routes
  3.7 0.9 copy.27.out_weight
  4.5 1.2 %copy.25.decay_down = bf16[2048,64]{1,0:T(8,128)(2,1)S(1)} copy(bf16[2048,64]{0,1:T(8,128)(2,1)} %param.29) | data formatting | bytes 524288 | tf_op args[6]
  5.8 1.2 %copy.26.rate_down = bf16[2048,64]{1,0:T(8,128)(2,1)S(1)} copy(bf16[2048,64]{0,1:T(8,128)(2,1)} %param.32) | data formatting | bytes 524288 | tf_op args[9]
  7.0 1.6 %copy-done = f32[16,8,4096]{2,1,0:T(8,128)S(1)} copy-done((f32[16,8,4096]{2,1,0:T(8,128)S(1)}, f32[16,8,4096]{2,1,0:T(8,128)}, u32[]{:S(2)}) %copy-start) | copy-done | bytes 2097176
  8.6 0.8 copy-done.1
  9.4 0.8 copy-done.2
  10.3 0.8 copy-done.3
  11.1 0.8 copy-done.4
  11.9 0.8 copy-done.5
  12.6 0.8 copy-done.6
  13.4 0.7 copy-done.7
  14.1 0.7 copy-done.8
  14.8 0.7 copy-done.9
  15.5 0.7 copy-done.10
  16.2 0.7 copy-done.11
  16.9 0.7 copy-done.12
  17.6 0.7 copy-done.13
  18.2 92.6 %shard_map.230 = (bf16[16,2048]{1,0:T(8,128)(2,1)S(1)}, f32[16,8,4096]{2,1,0:T(8,128)S(1)}) custom-call(bf16[16,2048]{1,0:T(8,128)(2,1)S(1)} %copy-done.1, f32[16,8,4096]{2,1,0:T(8,128)S(1)} %copy-done, f32[1,2048]{1,0:T(1,128)S(1)} %bitcast.8, bf16[32,512]{1,0:T(8,128)(2,1)S(1)} %copy-done.4, bf16[32,512]{1,0:T(8,128)(2,1)S(1)} %copy-done.5, ...), custom_call_target="tpu_custom_call" | custom-call | tf_op jit(solution)/shard_map/pallas_call | solution.py:579
  110.8 0.6 copy.32
  111.5 1.3 %copy.33 = f32[16,8,4096]{2,1,0:T(8,128)} copy(f32[16,8,4096]{2,1,0:T(8,128)S(1)} %get-tuple-element.5) | data formatting | bytes 4194304
  (14 shorter events, 0.0 us)
Async XLA Ops:
  7.0 1.6 %copy-start = (f32[16,8,4096]{2,1,0:T(8,128)S(1)}, f32[16,8,4096]{2,1,0:T(8,128)}, u32[]{:S(2)}) copy-start(f32[16,8,4096]{2,1,0:T(8,128)} %state_in.1) | copy-start | bytes 6291460
  8.6 0.8 copy-start.1
  9.4 0.8 copy-start.2
  10.3 0.8 copy-start.3
  11.1 0.8 copy-start.4
  11.9 0.8 copy-start.5
  12.6 0.8 copy-start.6
  13.4 0.7 copy-start.7
  14.1 0.7 copy-start.8
  14.8 0.7 copy-start.9
  15.5 0.7 copy-start.10
  16.2 0.7 copy-start.11
  16.9 0.7 copy-start.12
  17.5 0.7 copy-start.13

commit v2 on v1

v2 whole, which is shorter than its diff:
```python
import functools

import jax
import jax.numpy as jnp
from jax import lax
from jax.experimental import pallas as pl
from jax.experimental.pallas import tpu as pltpu
from jax.sharding import PartitionSpec as P

MESH = pl.DeviceIdType.MESH
HEAD_DIM = 64
CAP = 2
LANES = 128
WIDE = 256

norm_eps = 1e-06
group_eps = 0.00064
clamp_limit = 7.0
gate_alpha = 1.702

F32 = jnp.float32
BF16 = jnp.bfloat16


def dot(a, b):
    return lax.dot_general(a, b, (((1,), (0,)), ((), ())), preferred_element_type=F32)


def dot_t(a, b):
    return lax.dot_general(a, b, (((1,), (1,)), ((), ())), preferred_element_type=F32)


def split(a):
    high = a.astype(BF16)
    return high, (a - high.astype(F32)).astype(BF16)


def dot_split(a, b):
    high, low = split(a)
    return dot(high, b) + dot(low, b)


def iota(shape, dim):
    return lax.broadcasted_iota(jnp.int32, shape, dim)


def one_hot(mask):
    return jnp.where(mask, 1.0, 0.0).astype(BF16)


def rms_scale(values, scales):
    return values * lax.rsqrt(jnp.mean(values * values, axis=-1, keepdims=True) + norm_eps) * scales


def kernel(
    n_ep,
    n_tp,
    layer_in_far,
    rec_weight_far,
    key_weight_far,
    val_weight_far,
    out_weight_t_far,
    mix_gain_far,
    decay_down_t_far,
    rate_down_t_far,
    decay_up_far,
    rate_up_far,
    decay_base_far,
    rate_base_far,
    key_scale_far,
    group_gain_far,
    routes_t_far,
    gates_t_far,
    post_gain_far,
    ffn_gain_far,
    out_gain_far,
    state_far,
    expert_gate_far,
    expert_up_far,
    expert_down_far,
    layer_out,
    new_state,
    layer_in,
    rec_weight,
    key_weight,
    val_weight,
    out_send,
    mix_gain,
    decay_down_t,
    rate_down_t,
    decay_up,
    rate_up,
    decay_base,
    rate_base,
    key_scale,
    group_gain,
    routes_t,
    gates_t,
    post_gain,
    ffn_gain,
    out_gain,
    state,
    w_gate,
    w_up,
    w_down,
    proj_send,
    proj_all,
    out_all,
    rows_all,
    normed_all,
    qkv_send,
    qkv_all,
    decay_rows,
    rate_rows,
    by_head,
    gather_all,
    pick_all,
    read_send,
    read_all,
    part_send,
    part_all,
    mix_rows,
    wide_rows,
    slot_send,
    slot_here,
    slot_far_send,
    slot_far,
    slot_all,
    down_send,
    down_all,
    back_send,
    back_all,
    back_far_send,
    back_far,
    moe_send,
    moe_all,
    load_sem,
    send_sem,
    recv_sem,
    proj_sem,
    slot_sem,
):
    far = (
        layer_in_far,
        rec_weight_far,
        key_weight_far,
        val_weight_far,
        out_weight_t_far,
        mix_gain_far,
        decay_down_t_far,
        rate_down_t_far,
        decay_up_far,
        rate_up_far,
        decay_base_far,
        rate_base_far,
        key_scale_far,
        group_gain_far,
        routes_t_far,
        gates_t_far,
        post_gain_far,
        ffn_gain_far,
        out_gain_far,
        state_far,
        expert_gate_far.at[0],
        expert_up_far.at[0],
        expert_down_far.at[0],
    )
    near = (
        layer_in,
        rec_weight,
        key_weight,
        val_weight,
        out_send,
        mix_gain,
        decay_down_t,
        rate_down_t,
        decay_up,
        rate_up,
        decay_base,
        rate_base,
        key_scale,
        group_gain,
        routes_t,
        gates_t,
        post_gain,
        ffn_gain,
        out_gain,
        state,
        w_gate,
        w_up,
        w_down,
    )
    loads = [pltpu.make_async_copy(a, b, load_sem.at[n]) for n, (a, b) in enumerate(zip(far, near))]
    first_big = len(loads) - 4
    seqs, width = layer_in.shape
    heads = state.shape[1]
    plane = heads
    n_z = n_ep // plane
    quarter = width // n_tp
    tiles = quarter // LANES
    slab = CAP * tiles
    rows = seqs * heads
    depth = rec_weight.shape[0]
    out_cols = out_send.shape[0]

    for load in loads[:first_big]:
        load.start()

    me = lax.axis_index("ep")
    mine = lax.axis_index("tp")
    member = lax.rem(me, plane)
    base = me - member

    def member_at(step):
        return lax.rem(member + step, plane)

    def z_at(step):
        return lax.rem(me + step * plane, n_ep)

    def tp_at(step):
        return lax.rem(mine + step, n_tp)

    def send(src, dst, phase, ep, tp, sem=None):
        pltpu.make_async_remote_copy(
            src_ref=src,
            dst_ref=dst,
            send_sem=send_sem.at[phase],
            recv_sem=recv_sem.at[phase] if sem is None else sem,
            device_id={"ep": ep, "tp": tp},
            device_id_type=MESH,
        ).start()

    def keep(src, dst, sem):
        pltpu.make_async_copy(src, dst, sem).start()

    def arrive(buffer, sem):
        pltpu.make_async_copy(buffer, buffer, sem).wait()

    def sent(buffer, phase):
        pltpu.make_async_copy(buffer, buffer, send_sem.at[phase]).wait()

    def loop(start, stop, body):
        def step(i, carry):
            body(i)
            return carry

        lax.fori_loop(start, stop, step, 0)

    barrier = pltpu.get_barrier_semaphore()

    def others(body):
        for k in range(n_z):
            away = n_z // 2 + (k + 1) // 2 * (1 if k % 2 else -1)
            first = lax.rem(base + away % n_z * plane, n_ep)
            loop(0 if away % n_z else 1, plane, lambda i, first=first: body(first + member_at(i)))

    def greet(to):
        pl.semaphore_signal(barrier, inc=1, device_id={"ep": to, "tp": mine}, device_id_type=MESH)

    others(greet)

    def greet_plane(i):
        pl.semaphore_signal(
            barrier,
            inc=1,
            device_id={"ep": base + member_at(lax.rem(i, plane)), "tp": tp_at(i // plane)},
            device_id_type=MESH,
        )

    loop(plane, plane * n_tp, greet_plane)

    for load in loads[:5]:
        load.wait()
    for h in range(heads):
        cut = slice(h * HEAD_DIM, (h + 1) * HEAD_DIM)
        proj_send[h, :depth, :] = jnp.concatenate([rec_weight[:, cut], key_weight[:, cut]], axis=1)
        proj_send[h, depth:, :] = jnp.concatenate(
            [val_weight[: depth // 2, cut], val_weight[depth // 2 :, cut]], axis=1
        )
    for load in loads[first_big:]:
        load.start()
    for load in loads[5:first_big]:
        load.wait()
    pl.semaphore_wait(barrier, n_ep - 1 + plane * (n_tp - 1))

    keep(proj_send.at[member], proj_all.at[me], proj_sem.at[0])

    def send_proj(i, away):
        to = member_at(i)
        at = lax.rem(base + (n_z + away) * plane, n_ep) + to
        send(proj_send.at[to], proj_all.at[me], 1, at, mine, proj_sem.at[(n_z - away) % n_z])

    for away in (2, -2):
        loop(0, plane, functools.partial(send_proj, away=away))
    chip, core = member // 2, lax.rem(member, 2)
    keep(layer_in, rows_all.at[chip, core], recv_sem.at[0])

    def send_rows(i):
        send(layer_in, rows_all.at[chip, core], 0, base + member_at(2 * i), mine)

    loop(1, plane // 2, send_rows)
    for away in (1, -1):
        loop(0, plane, functools.partial(send_proj, away=away))
    loop(1, plane, functools.partial(send_proj, away=0))
    z_me = me // plane

    own_normed = rms_scale(layer_in[...].astype(F32), mix_gain[...]).astype(BF16)
    decay_hidden = jnp.tanh(dot_t(own_normed, decay_down_t[...])).astype(BF16)
    rate_hidden = dot_t(own_normed, rate_down_t[...]).astype(BF16)
    decay_sig = jax.nn.sigmoid(decay_base[...] + dot(decay_hidden, decay_up[...]))
    decay = jnp.exp(-jnp.exp(jnp.full((), -0.5, F32)) * decay_sig)
    rate = jax.nn.sigmoid(rate_base[...] + dot(rate_hidden, rate_up[...]))
    for h in range(heads):
        cut = slice(h * HEAD_DIM, (h + 1) * HEAD_DIM)
        decay_rows[h * seqs : (h + 1) * seqs, :] = decay[:, cut]
        rate_rows[h * seqs : (h + 1) * seqs, :] = rate[:, cut]
        by_head[0, h : h + 1, :] = key_scale[:, cut]
        by_head[1, h : h + 1, :] = group_gain[:, cut]

    top = routes_t.shape[0]
    named_t = jnp.zeros((n_ep, seqs), F32)
    weight_t = jnp.zeros((n_ep, seqs), F32)
    for j in range(top):
        hit = iota((n_ep, seqs), 0) == routes_t[j : j + 1, :]
        named_t += jnp.where(hit, 1.0, 0.0)
        weight_t += jnp.where(hit, gates_t[j : j + 1, :], 0.0)
    before_t = dot(named_t.astype(BF16), one_hot(iota((seqs, seqs), 0) < iota((seqs, seqs), 1)))
    eye = one_hot(iota((seqs, seqs), 0) == iota((seqs, seqs), 1))
    combine = []
    for s in range(CAP):
        high, low = split(jnp.where(before_t == float(s), weight_t, 0.0))
        combine.append((dot_t(eye, high).astype(BF16), dot_t(eye, low).astype(BF16)))
    per = WIDE // HEAD_DIM

    def tables(i):
        block = pl.ds(pl.multiple_of(i * WIDE, WIDE), WIDE)
        pick_all[:, block] = one_hot(
            iota((HEAD_DIM, WIDE), 0) == i * per + iota((HEAD_DIM, WIDE), 1) // HEAD_DIM
        )
        gather_all[block, :] = one_hot(
            iota((WIDE, HEAD_DIM), 1) == i * per + iota((WIDE, HEAD_DIM), 0) // HEAD_DIM
        )

    loop(0, HEAD_DIM // per, tables)

    def plane_of(away):
        at = lax.rem(base + (n_z + away) * plane, n_ep)
        return at, proj_all.at[pl.ds(at, plane)]

    half = plane // 2
    for away in (-2, 2):
        at, blocks = plane_of(away)
        arrive(blocks, proj_sem.at[away % n_z])
        side = -away // 2
        to = lax.rem(base + (n_z + side) * plane, n_ep) + member
        send(blocks, blocks, 1, to, mine, proj_sem.at[(away - side) % n_z])
        part = proj_all.at[pl.ds(at + (0 if side > 0 else half), half)]
        to = lax.rem(base + (n_z + 2 * side) * plane, n_ep) + member
        send(part, part, 1, to, mine, proj_sem.at[(away - 2 * side) % n_z])
    arrive(rows_all.at[:, core], recv_sem.at[0])
    sibling = me + 1 - 2 * core
    send(rows_all.at[:, core], rows_all.at[:, core], 13, sibling, mine)
    keep(out_send, out_all.at[z_me], recv_sem.at[2])

    def send_out(i):
        send(out_send, out_all.at[z_me], 2, z_at(i), mine)

    loop(1, n_z, send_out)

    arrive(rows_all.at[:, 1 - core], recv_sem.at[13])

    def norm_rows(i):
        values = rms_scale(rows_all[i // 2, lax.rem(i, 2)].astype(F32), mix_gain[...]).astype(BF16)
        normed_all[pl.ds(pl.multiple_of(i * seqs, seqs), seqs), :] = values

    loop(0, plane, norm_rows)

    for away in (0, 1, -1, 3, -3, 4):
        arrive(plane_of(away)[1], proj_sem.at[away % n_z])
    pairs = proj_all[:, :depth, :].reshape(n_ep * depth, 2 * HEAD_DIM)
    vals = proj_all[:, depth:, :]
    vals = jnp.concatenate([vals, vals], axis=1).reshape(n_ep * depth, 2 * HEAD_DIM)
    spread = (n_ep * depth, 2 * HEAD_DIM)
    first = lax.rem(iota(spread, 0), depth) < depth // 2
    vals = jnp.where(first == (iota(spread, 1) < HEAD_DIM), vals.astype(F32), 0.0).astype(BF16)
    normed = normed_all[...]
    pair_sum = dot(normed, pairs)
    val_sum = dot(normed, vals)
    val_sum = val_sum[:, :HEAD_DIM] + val_sum[:, HEAD_DIM:]
    together = jnp.concatenate([pair_sum, val_sum, jnp.zeros_like(val_sum)], axis=1)
    qkv_send[...] = together.astype(BF16).reshape(plane, seqs, WIDE)
    keep(qkv_send.at[member], qkv_all.at[member], recv_sem.at[3])

    def send_qkv(i):
        to = member_at(i)
        send(qkv_send.at[to], qkv_all.at[member], 3, base + to, mine)

    loop(1, plane, send_qkv)

    turn = one_hot(
        iota((rows, rows), 1)
        == lax.rem(iota((rows, rows), 0), heads) * seqs + iota((rows, rows), 0) // heads
    )
    turn_back = one_hot(
        iota((rows, rows), 1)
        == lax.rem(iota((rows, rows), 0), seqs) * heads + iota((rows, rows), 0) // seqs
    )
    decay_high, decay_low = split(decay_rows[...])
    rate_high, rate_low = split(rate_rows[...])
    turned = dot(turn, jnp.concatenate([decay_high, decay_low, rate_high, rate_low], axis=1))
    decay = turned[:, :HEAD_DIM] + turned[:, HEAD_DIM : 2 * HEAD_DIM]
    rate = turned[:, 2 * HEAD_DIM : 3 * HEAD_DIM] + turned[:, 3 * HEAD_DIM :]

    arrive(qkv_all, recv_sem.at[3])
    qkv = dot(turn, qkv_all[...].reshape(rows, WIDE))
    rec = qkv[:, :HEAD_DIM]
    key = qkv[:, HEAD_DIM : 2 * HEAD_DIM]
    val = qkv[:, 2 * HEAD_DIM : 3 * HEAD_DIM].astype(BF16)

    def of_heads(n):
        return jnp.broadcast_to(by_head[n][None], (seqs, heads, HEAD_DIM)).reshape(rows, HEAD_DIM)

    scaled = key * of_heads(0)
    unit = scaled * lax.rsqrt(jnp.sum(scaled * scaled, axis=-1, keepdims=True) + norm_eps)

    def wide(a):
        return jnp.concatenate([a] * (WIDE // HEAD_DIM), axis=1)

    unit_w, read_w = wide(unit), wide(decay * rec)
    loads[first_big].wait()

    def sums(i, totals):
        for k in range(4):
            block = pl.ds(pl.multiple_of((i * 4 + k) * WIDE, WIDE), WIDE)
            old = state[:, :, block].reshape(rows, WIDE)
            stacked = jnp.concatenate(split(old * unit_w) + split(old * read_w), axis=0)
            totals += dot(stacked, gather_all[block, :])
        return totals

    totals = lax.fori_loop(0, HEAD_DIM // per // 4, sums, jnp.zeros((4 * rows, HEAD_DIM), F32))
    along = totals[:rows] + totals[rows : 2 * rows]
    along_read = jnp.sum(unit * rate * rec, axis=-1, keepdims=True)
    val_read = jnp.sum(key * rate * rec, axis=-1, keepdims=True)
    readout = totals[2 * rows : 3 * rows] + totals[3 * rows :] - along * along_read + val.astype(F32) * val_read
    centred = readout - jnp.mean(readout, axis=-1, keepdims=True)
    normed_out = centred * lax.rsqrt(jnp.mean(centred * centred, axis=-1, keepdims=True) + group_eps)
    normed_out = dot(turn_back, (normed_out * of_heads(1)).astype(BF16)).astype(BF16)
    for h in range(heads):
        read_send[:, h * HEAD_DIM : (h + 1) * HEAD_DIM] = normed_out[h * seqs : (h + 1) * seqs, :]
    keep(read_send, read_all.at[member], recv_sem.at[4])

    def send_read(i):
        send(read_send, read_all.at[member], 4, base + member_at(i), mine)

    loop(1, plane, send_read)

    decay_w, unit_rate, key_rate = wide(decay), wide(unit * rate), wide(key * rate)
    along_high, along_low = split(along)
    spread_rows = jnp.concatenate([along_high, along_low, val], axis=0)

    def update(i):
        for k in range(2):
            block = pl.ds(pl.multiple_of((i * 2 + k) * WIDE, WIDE), WIDE)
            wider = dot(spread_rows, pick_all[:, block])
            old = state[:, :, block].reshape(rows, WIDE)
            new = old * decay_w - (wider[:rows] + wider[rows : 2 * rows]) * unit_rate
            new += wider[2 * rows :] * key_rate
            new_state[:, :, block] = new.reshape(seqs, heads, WIDE)

    loop(0, HEAD_DIM // per // 2, update)

    arrive(out_all, recv_sem.at[2])
    arrive(read_all, recv_sem.at[4])
    part = dot_t(
        read_all[...].reshape(plane * seqs, quarter), out_all[...].reshape(n_z * out_cols, quarter)
    )
    part_send[...] = part.astype(BF16).reshape(plane, seqs, n_z * out_cols)
    keep(part_send.at[member], part_all.at[mine * plane + member], recv_sem.at[5])

    def send_part(i):
        to = member_at(lax.rem(i, plane))
        send(part_send.at[to], part_all.at[mine * plane + member], 5, base + to, tp_at(i // plane))

    loop(1, plane * n_tp, send_part)

    arrive(part_all, recv_sem.at[5])
    for g in range(plane):
        total = part_all[g].astype(F32)
        for t in range(1, n_tp):
            total += part_all[t * plane + g].astype(F32)
        for z in range(n_z):
            at = (z * plane + g) * out_cols
            mix_rows[:, at : at + out_cols] = total[:, z * out_cols : (z + 1) * out_cols]
    middle = (layer_in[...].astype(F32) + rms_scale(mix_rows[...], post_gain[...])).astype(BF16)
    mix_rows[...] = middle.astype(F32)
    ffn_in = rms_scale(mix_rows[...], ffn_gain[...])

    mix_rows[...] = ffn_in
    opposite = tp_at(n_tp // 2)

    def to_slabs(values, dst):
        for s in range(CAP):
            for t in range(tiles):
                wide_rows[pl.ds(s * tiles + t, n_ep, stride=slab), :] = values[s][:, t * LANES : (t + 1) * LANES]
        dst[...] = wide_rows[...].astype(BF16).reshape(n_ep, slab, LANES)

    def to_everyone(src, dst, phase):
        keep(src.at[me], dst.at[me], recv_sem.at[phase])

        others(lambda to: send(src.at[to], dst.at[me], phase, to, mine))

    for at, src, dst, phase in ((mine, slot_send, slot_here, 6), (opposite, slot_far_send, slot_far, 11)):
        cut = mix_rows[:, pl.ds(pl.multiple_of(at * quarter, quarter), quarter)].astype(BF16)
        to_slabs(
            [dot(jnp.where(before_t == float(s), named_t, 0.0).astype(BF16), cut) for s in range(CAP)], src
        )
        to_everyone(src, dst, phase)
    mix_rows[...] = middle.astype(F32)

    arrive(slot_here, recv_sem.at[6])
    sides = (1, n_tp - 1)
    for step in sides:
        send(slot_here, slot_all.at[mine], 7, me, tp_at(step), slot_sem.at[mine])
    loads[first_big + 1].wait()
    loads[first_big + 2].wait()

    def from_slabs(source):
        wide_rows[...] = source.astype(F32).reshape(n_ep * slab, LANES)
        return [
            [wide_rows[pl.ds(s * tiles + t, n_ep, stride=slab), :] for t in range(tiles)]
            for s in range(CAP)
        ]

    gate = up = None
    for step in (0, n_tp // 2) + sides:
        at = tp_at(step)
        if step == 0:
            source = slot_here[...]
        elif step == n_tp // 2:
            arrive(slot_far, recv_sem.at[11])
            source = slot_far[...]
        else:
            arrive(slot_all.at[at], slot_sem.at[at])
            source = slot_all[at]
        part = jnp.concatenate([jnp.concatenate(p, axis=1) for p in from_slabs(source)], axis=0).astype(BF16)
        feats = pl.ds(pl.multiple_of(at * quarter, quarter), quarter)
        gate_part, up_part = dot(part, w_gate[feats, :]), dot(part, w_up[feats, :])
        gate = gate_part if gate is None else gate + gate_part
        up = up_part if up is None else up + up_part
    gate = jnp.minimum(gate, clamp_limit)
    up = jnp.clip(up, -clamp_limit, clamp_limit)
    hidden = ((up + 1.0) * gate * jax.nn.sigmoid(gate_alpha * gate)).astype(BF16)

    loads[first_big + 3].wait()

    def down(at):
        return dot(hidden, w_down[:, pl.ds(pl.multiple_of(at * quarter, quarter), quarter)]).astype(BF16)

    def slabs_back(values, src, dst, phase):
        to_slabs([values[s * n_ep : (s + 1) * n_ep] for s in range(CAP)], src)
        to_everyone(src, dst, phase)

    for step in sides:
        at = tp_at(step)
        down_send[at] = down(at)
        send(down_send.at[at], down_all.at[mine], 8, me, at, slot_sem.at[n_tp + mine])
    slabs_back(down(opposite).astype(F32), back_far_send, back_far, 12)
    total = down(mine).astype(F32)
    for step in sides:
        at = tp_at(step)
        arrive(down_all.at[at], slot_sem.at[n_tp + at])
        total += down_all[at].astype(F32)
    slabs_back(total, back_send, back_all, 9)

    for n, (buffer, phase) in enumerate(((back_far, 12), (back_all, 9))):
        arrive(buffer, recv_sem.at[phase])
        moe = jnp.zeros((seqs, quarter), F32)
        for (high, low), p in zip(combine, from_slabs(buffer[...])):
            values = jnp.concatenate(p, axis=1).astype(BF16)
            moe += dot(high, values) + dot(low, values)
        moe_send[n] = moe.astype(BF16)
        last = 14 if n == 0 else 10
        keep(moe_send.at[n], moe_all.at[n, mine], recv_sem.at[last])
        for step in range(1, n_tp):
            send(moe_send.at[n], moe_all.at[n, mine], last, me, tp_at(step))
    arrive(moe_all.at[0], recv_sem.at[14])
    arrive(moe_all.at[1], recv_sem.at[10])
    moe = jnp.concatenate(
        [moe_all[1, t].astype(F32) + moe_all[0, (t + n_tp // 2) % n_tp].astype(F32) for t in range(n_tp)], axis=1
    )
    layer_out[...] = (mix_rows[...] + rms_scale(moe, out_gain[...])).astype(BF16)

    sent(rows_all.at[pl.ds(0, plane // 2 - 1), 0], 0)
    sent(rows_all.at[:, core], 13)
    sent(moe_all.at[0, pl.ds(0, n_tp - 1)], 14)
    sent(proj_all.at[pl.ds(0, n_ep - 1)], 1)
    sent(out_all.at[pl.ds(0, n_z - 1)], 2)
    sent(slot_far.at[pl.ds(0, n_ep - 1)], 11)
    sent(back_far.at[pl.ds(0, n_ep - 1)], 12)
    sent(qkv_all.at[pl.ds(0, plane - 1)], 3)
    sent(read_all.at[pl.ds(0, plane - 1)], 4)
    sent(part_all.at[pl.ds(0, n_tp * plane - 1)], 5)
    sent(slot_here.at[pl.ds(0, n_ep - 1)], 6)
    sent(slot_all.at[pl.ds(0, 2)], 7)
    sent(down_all.at[pl.ds(0, 2)], 8)
    sent(back_all.at[pl.ds(0, n_ep - 1)], 9)
    sent(moe_all.at[1, pl.ds(0, n_tp - 1)], 10)


def local(n_ep, n_tp, *args):
    (
        layer_in,
        state_in,
        mix_gain,
        rec_weight,
        key_weight,
        val_weight,
        decay_down,
        decay_up,
        decay_base,
        rate_down,
        rate_up,
        rate_base,
        key_scale,
        group_gain,
        out_weight,
        post_gain,
        ffn_gain,
        routes,
        route_gates,
        expert_gate,
        expert_up,
        expert_down,
        out_gain,
    ) = args
    seqs, width = layer_in.shape
    heads = state_in.shape[1]
    plane = heads
    n_z = n_ep // plane
    quarter = width // n_tp
    slab = CAP * (quarter // LANES)
    depth = rec_weight.shape[0]
    out_cols = out_weight.shape[1]
    slots = CAP * n_ep
    state_lanes = state_in.shape[2]
    row = lambda a: a.reshape(1, -1)
    operands = (
        layer_in,
        rec_weight,
        key_weight,
        val_weight,
        out_weight.T,
        row(mix_gain),
        decay_down.T,
        rate_down.T,
        decay_up,
        rate_up,
        row(decay_base),
        row(rate_base),
        row(key_scale),
        row(group_gain),
        routes.T,
        route_gates.T,
        row(post_gain),
        row(ffn_gain),
        row(out_gain),
        state_in,
        expert_gate,
        expert_up,
        expert_down,
    )
    far = pl.BlockSpec(memory_space=pltpu.HBM)
    local_shapes = [a.shape[1:] if a.ndim == 3 and n >= len(operands) - 3 else a.shape for n, a in enumerate(operands)]
    scratch = [pltpu.VMEM(shape, a.dtype) for shape, a in zip(local_shapes, operands)]
    scratch += [
        pltpu.VMEM((plane, depth + depth // 2, 2 * HEAD_DIM), BF16),
        pltpu.VMEM((n_ep, depth + depth // 2, 2 * HEAD_DIM), BF16),
        pltpu.VMEM((n_z, out_cols, quarter), BF16),
        pltpu.VMEM((plane // 2, 2, seqs, width), BF16),
        pltpu.VMEM((plane * seqs, width), BF16),
        pltpu.VMEM((plane, seqs, WIDE), BF16),
        pltpu.VMEM((plane, seqs, WIDE), BF16),
        pltpu.VMEM((heads * seqs, HEAD_DIM), F32),
        pltpu.VMEM((heads * seqs, HEAD_DIM), F32),
        pltpu.VMEM((2, heads, HEAD_DIM), F32),
        pltpu.VMEM((HEAD_DIM * HEAD_DIM, HEAD_DIM), BF16),
        pltpu.VMEM((HEAD_DIM, HEAD_DIM * HEAD_DIM), BF16),
        pltpu.VMEM((seqs, quarter), BF16),
        pltpu.VMEM((plane, seqs, quarter), BF16),
        pltpu.VMEM((plane, seqs, n_z * out_cols), BF16),
        pltpu.VMEM((n_tp * plane, seqs, n_z * out_cols), BF16),
        pltpu.VMEM((seqs, width), F32),
        pltpu.VMEM((n_ep * slab, LANES), F32),
        pltpu.VMEM((n_ep, slab, LANES), BF16),
        pltpu.VMEM((n_ep, slab, LANES), BF16),
        pltpu.VMEM((n_ep, slab, LANES), BF16),
        pltpu.VMEM((n_ep, slab, LANES), BF16),
        pltpu.VMEM((n_tp, n_ep, slab, LANES), BF16),
        pltpu.VMEM((n_tp, slots, quarter), BF16),
        pltpu.VMEM((n_tp, slots, quarter), BF16),
        pltpu.VMEM((n_ep, slab, LANES), BF16),
        pltpu.VMEM((n_ep, slab, LANES), BF16),
        pltpu.VMEM((n_ep, slab, LANES), BF16),
        pltpu.VMEM((n_ep, slab, LANES), BF16),
        pltpu.VMEM((2, seqs, quarter), BF16),
        pltpu.VMEM((2, n_tp, seqs, quarter), BF16),
        pltpu.SemaphoreType.DMA((len(operands),)),
        pltpu.SemaphoreType.DMA((15,)),
        pltpu.SemaphoreType.DMA((15,)),
        pltpu.SemaphoreType.DMA((n_z,)),
        pltpu.SemaphoreType.DMA((2 * n_tp,)),
    ]
    return pl.pallas_call(
        functools.partial(kernel, n_ep, n_tp),
        out_shape=(
            jax.ShapeDtypeStruct(layer_in.shape, BF16),
            jax.ShapeDtypeStruct((seqs, heads, state_lanes), F32),
        ),
        in_specs=[far] * len(operands),
        out_specs=[pl.BlockSpec(memory_space=pltpu.VMEM)] * 2,
        scratch_shapes=scratch,
        compiler_params=pltpu.CompilerParams(
            collective_id=0, has_side_effects=True, vmem_limit_bytes=32 * 1024 * 1024
        ),
    )(*[pltpu.with_memory_space_constraint(a, pltpu.HBM) for a in operands])


def solution(mesh):
    in_specs = (
        P("ep", None),
        P("ep", "tp", None),
        P(),
        P("ep", "tp"),
        P("ep", "tp"),
        P("ep", "tp"),
        P(),
        P(None, "tp"),
        P("tp"),
        P(),
        P(None, "tp"),
        P("tp"),
        P("tp"),
        P("tp"),
        P("tp", "ep"),
        P(),
        P(),
        P("ep", None),
        P("ep", None),
        P("ep", None, "tp"),
        P("ep", None, "tp"),
        P("ep", "tp", None),
        P(),
    )
    out_specs = (P("ep", None), P("ep", "tp", None))
    body = functools.partial(local, mesh.shape["ep"], mesh.shape["tp"])
    return jax.shard_map(body, mesh=mesh, in_specs=in_specs, out_specs=out_specs, check_vma=False)
```

time: 114 us -> 79.6 us (0.70)
  local copies, waits for them, and re-layouts: 19.5 us -> 1.95 us
  Pallas kernels: 92.6 us -> 76.9 us
    unnamed x35 -> x2, local copies, waits for them, and re-layouts: 18 us -> 1.95 us
    pallas_call x1, Pallas kernels: 92.6 us -> 76.9 us  [local(): pl.pallas_call(functools.partial(kernel, n_ep, n_tp), out_shape=(jax.Shap...]
    reshape x2 -> x0, local copies, waits for them, and re-layouts: 1.51 us -> none  [local(): by_head = lambda a: a.reshape(heads, HEAD_DIM)]
where the time goes in v2:
time: 79.6 us; the launch traced here: 79.5 us
  Pallas kernels  76.9 us (97%)
  local copies, waits for them, and re-layouts  1.95 us (2%)
    pallas_call x1, Pallas kernels, local(): pl.pallas_call(functools.partial(kernel, n_ep, n_tp), out_shape=(jax.Shap...  76.9 us
    unnamed x2, local copies, waits for them, and re-layouts  1.95 us

profile of v2, /device:TPU:1, one launch (start us, length us, event | category | flops | bytes accessed | tf_op | source)
XLA Modules:
  0.0 79.5 jit_solution(16011167565198462439)
XLA Ops:
  0.6 76.9 %shard_map.230 = (bf16[16,2048]{1,0:T(8,128)(2,1)S(1)}, f32[16,8,4096]{2,1,0:T(8,128)S(1)}) custom-call(bf16[16,2048]{1,0:T(8,128)(2,1)} %layer_in_far.1, bf16[32,512]{1,0:T(8,128)(2,1)} %rec_weight_far.1, bf16[32,512]{1,0:T(8,128)(2,1)} %key_weight_far.1, bf16[32,512]{1,0:T(8,128)(2,1)} %val_weight_far.1, bf16[32,512]{1,0:T(8,128)(2,1)} %bitcast.15, ...), custom_call_target="tpu_custom_call" | custom-call | tf_op jit(solution)/shard_map/pallas_call | solution.py:713
  77.6 0.6 copy.27
  78.2 1.3 %copy.28 = f32[16,8,4096]{2,1,0:T(8,128)} copy(f32[16,8,4096]{2,1,0:T(8,128)S(1)} %get-tuple-element.5) | data formatting | bytes 4194304

commit v3 on v2

--- a/solution.py
+++ b/solution.py
@@ -103,13 +103,17 @@
     w_gate,
     w_up,
     w_down,
-    proj_send,
-    proj_all,
+    pair_send,
+    pair_all,
+    val_send,
+    val_all,
     out_all,
     rows_all,
     normed_all,
-    qkv_send,
-    qkv_all,
+    pair_out,
+    pair_in,
+    val_out,
+    val_in,
     decay_rows,
     rate_rows,
     by_head,
@@ -137,8 +141,11 @@
     load_sem,
     send_sem,
     recv_sem,
-    proj_sem,
+    pair_sem,
+    val_sem,
+    near_sem,
     slot_sem,
+    down_sem,
 ):
     far = (
         layer_in_far,
@@ -252,9 +259,13 @@
         for k in range(n_z):
             away = n_z // 2 + (k + 1) // 2 * (1 if k % 2 else -1)
             first = lax.rem(base + away % n_z * plane, n_ep)
-            loop(0 if away % n_z else 1, plane, lambda i, first=first: body(first + member_at(i)))
-
-    def greet(to):
+            loop(
+                0 if away % n_z else 1,
+                plane,
+                lambda i, first=first, away=away: body(first + member_at(i), away),
+            )
+
+    def greet(to, away):
         pl.semaphore_signal(barrier, inc=1, device_id={"ep": to, "tp": mine}, device_id_type=MESH)
 
     others(greet)
@@ -273,8 +284,8 @@
         load.wait()
     for h in range(heads):
         cut = slice(h * HEAD_DIM, (h + 1) * HEAD_DIM)
-        proj_send[h, :depth, :] = jnp.concatenate([rec_weight[:, cut], key_weight[:, cut]], axis=1)
-        proj_send[h, depth:, :] = jnp.concatenate(
+        pair_send[h] = jnp.concatenate([rec_weight[:, cut], key_weight[:, cut]], axis=1)
+        val_send[h] = jnp.concatenate(
             [val_weight[: depth // 2, cut], val_weight[depth // 2 :, cut]], axis=1
         )
     for load in loads[first_big:]:
@@ -283,15 +294,23 @@
         load.wait()
     pl.semaphore_wait(barrier, n_ep - 1 + plane * (n_tp - 1))
 
-    keep(proj_send.at[member], proj_all.at[me], proj_sem.at[0])
-
-    def send_proj(i, away):
-        to = member_at(i)
-        at = lax.rem(base + (n_z + away) * plane, n_ep) + to
-        send(proj_send.at[to], proj_all.at[me], 1, at, mine, proj_sem.at[(n_z - away) % n_z])
+    keep(pair_send.at[member], pair_all.at[me], pair_sem.at[0])
+    keep(val_send.at[member], val_all.at[me], val_sem.at[0])
+    pair_wave = (pair_send, pair_all, 1, pair_sem)
+    val_wave = (val_send, val_all, 15, val_sem)
+
+    def send_wave(wave, away):
+        src, dst, phase, sem = wave
+        first = lax.rem(base + away % n_z * plane, n_ep)
+
+        def one(i):
+            to = member_at(i)
+            send(src.at[to], dst.at[me], phase, first + to, mine, sem.at[-away % n_z])
+
+        loop(0 if away else 1, plane, one)
 
     for away in (2, -2):
-        loop(0, plane, functools.partial(send_proj, away=away))
+        send_wave(pair_wave, away)
     chip, core = member // 2, lax.rem(member, 2)
     keep(layer_in, rows_all.at[chip, core], recv_sem.at[0])
 
@@ -299,9 +318,10 @@
         send(layer_in, rows_all.at[chip, core], 0, base + member_at(2 * i), mine)
 
     loop(1, plane // 2, send_rows)
-    for away in (1, -1):
-        loop(0, plane, functools.partial(send_proj, away=away))
-    loop(1, plane, functools.partial(send_proj, away=0))
+    for away in (1, -1, 0):
+        send_wave(pair_wave, away)
+    for away in (2, -2):
+        send_wave(val_wave, away)
     z_me = me // plane
 
     own_normed = rms_scale(layer_in[...].astype(F32), mix_gain[...]).astype(BF16)
@@ -343,23 +363,36 @@
 
     loop(0, HEAD_DIM // per, tables)
 
-    def plane_of(away):
-        at = lax.rem(base + (n_z + away) * plane, n_ep)
-        return at, proj_all.at[pl.ds(at, plane)]
+    def plane_of(buffer, away):
+        at = lax.rem(base + away % n_z * plane, n_ep)
+        return at, buffer.at[pl.ds(at, plane)]
 
     half = plane // 2
-    for away in (-2, 2):
-        at, blocks = plane_of(away)
-        arrive(blocks, proj_sem.at[away % n_z])
-        side = -away // 2
-        to = lax.rem(base + (n_z + side) * plane, n_ep) + member
-        send(blocks, blocks, 1, to, mine, proj_sem.at[(away - side) % n_z])
-        part = proj_all.at[pl.ds(at + (0 if side > 0 else half), half)]
-        to = lax.rem(base + (n_z + 2 * side) * plane, n_ep) + member
-        send(part, part, 1, to, mine, proj_sem.at[(away - 2 * side) % n_z])
+
+    def forward(wave):
+        _, buffer, phase, sem = wave
+        for away in (-2, 2):
+            at, blocks = plane_of(buffer, away)
+            arrive(blocks, sem.at[away % n_z])
+            side = -away // 2
+            to = lax.rem(base + side % n_z * plane, n_ep) + member
+            send(blocks, blocks, phase, to, mine, sem.at[(away - side) % n_z])
+            part = buffer.at[pl.ds(at + (0 if side > 0 else half), half)]
+            to = lax.rem(base + 2 * side % n_z * plane, n_ep) + member
+            send(part, part, phase, to, mine, sem.at[(away - 2 * side) % n_z])
+
+    def arrive_wave(wave):
+        _, buffer, _, sem = wave
+        for away in (0, 1, -1, 3, -3, 4):
+            arrive(plane_of(buffer, away)[1], sem.at[away % n_z])
+
+    forward(pair_wave)
+    for away in (1, -1, 0):
+        send_wave(val_wave, away)
     arrive(rows_all.at[:, core], recv_sem.at[0])
     sibling = me + 1 - 2 * core
     send(rows_all.at[:, core], rows_all.at[:, core], 13, sibling, mine)
+    forward(val_wave)
     keep(out_send, out_all.at[z_me], recv_sem.at[2])
 
     def send_out(i):
@@ -375,27 +408,33 @@
 
     loop(0, plane, norm_rows)
 
-    for away in (0, 1, -1, 3, -3, 4):
-        arrive(plane_of(away)[1], proj_sem.at[away % n_z])
-    pairs = proj_all[:, :depth, :].reshape(n_ep * depth, 2 * HEAD_DIM)
-    vals = proj_all[:, depth:, :]
+    arrive_wave(pair_wave)
+    normed = normed_all[...]
+    pair_sum = dot(normed, pair_all[...].reshape(n_ep * depth, 2 * HEAD_DIM))
+    pair_out[...] = pair_sum.astype(BF16).reshape(plane, seqs, 2 * HEAD_DIM)
+
+    def share(src, dst, phase):
+        keep(src.at[member], dst.at[member], recv_sem.at[phase])
+
+        def one(i):
+            to = member_at(i)
+            send(src.at[to], dst.at[member], phase, base + to, mine)
+
+        loop(1, plane, one)
+
+    share(pair_out, pair_in, 3)
+
+    arrive_wave(val_wave)
+    vals = val_all[...]
     vals = jnp.concatenate([vals, vals], axis=1).reshape(n_ep * depth, 2 * HEAD_DIM)
     spread = (n_ep * depth, 2 * HEAD_DIM)
     first = lax.rem(iota(spread, 0), depth) < depth // 2
     vals = jnp.where(first == (iota(spread, 1) < HEAD_DIM), vals.astype(F32), 0.0).astype(BF16)
-    normed = normed_all[...]
-    pair_sum = dot(normed, pairs)
     val_sum = dot(normed, vals)
     val_sum = val_sum[:, :HEAD_DIM] + val_sum[:, HEAD_DIM:]
-    together = jnp.concatenate([pair_sum, val_sum, jnp.zeros_like(val_sum)], axis=1)
-    qkv_send[...] = together.astype(BF16).reshape(plane, seqs, WIDE)
-    keep(qkv_send.at[member], qkv_all.at[member], recv_sem.at[3])
-
-    def send_qkv(i):
-        to = member_at(i)
-        send(qkv_send.at[to], qkv_all.at[member], 3, base + to, mine)
-
-    loop(1, plane, send_qkv)
+    val_sum = jnp.concatenate([val_sum, jnp.zeros_like(val_sum)], axis=1)
+    val_out[...] = val_sum.astype(BF16).reshape(plane, seqs, 2 * HEAD_DIM)
+    share(val_out, val_in, 16)
 
     turn = one_hot(
         iota((rows, rows), 1)
@@ -411,11 +450,10 @@
     decay = turned[:, :HEAD_DIM] + turned[:, HEAD_DIM : 2 * HEAD_DIM]
     rate = turned[:, 2 * HEAD_DIM : 3 * HEAD_DIM] + turned[:, 3 * HEAD_DIM :]
 
-    arrive(qkv_all, recv_sem.at[3])
-    qkv = dot(turn, qkv_all[...].reshape(rows, WIDE))
-    rec = qkv[:, :HEAD_DIM]
-    key = qkv[:, HEAD_DIM : 2 * HEAD_DIM]
-    val = qkv[:, 2 * HEAD_DIM : 3 * HEAD_DIM].astype(BF16)
+    arrive(pair_in, recv_sem.at[3])
+    pair = dot(turn, pair_in[...].reshape(rows, 2 * HEAD_DIM))
+    rec = pair[:, :HEAD_DIM]
+    key = pair[:, HEAD_DIM:]
 
     def of_heads(n):
         return jnp.broadcast_to(by_head[n][None], (seqs, heads, HEAD_DIM)).reshape(rows, HEAD_DIM)
@@ -441,6 +479,8 @@
     along = totals[:rows] + totals[rows : 2 * rows]
     along_read = jnp.sum(unit * rate * rec, axis=-1, keepdims=True)
     val_read = jnp.sum(key * rate * rec, axis=-1, keepdims=True)
+    arrive(val_in, recv_sem.at[16])
+    val = dot(turn, val_in[...].reshape(rows, 2 * HEAD_DIM))[:, :HEAD_DIM].astype(BF16)
     readout = totals[2 * rows : 3 * rows] + totals[3 * rows :] - along * along_read + val.astype(F32) * val_read
     centred = readout - jnp.mean(readout, axis=-1, keepdims=True)
     normed_out = centred * lax.rsqrt(jnp.mean(centred * centred, axis=-1, keepdims=True) + group_eps)
@@ -504,23 +544,30 @@
                 wide_rows[pl.ds(s * tiles + t, n_ep, stride=slab), :] = values[s][:, t * LANES : (t + 1) * LANES]
         dst[...] = wide_rows[...].astype(BF16).reshape(n_ep, slab, LANES)
 
-    def to_everyone(src, dst, phase):
-        keep(src.at[me], dst.at[me], recv_sem.at[phase])
-
-        others(lambda to: send(src.at[to], dst.at[me], phase, to, mine))
-
-    for at, src, dst, phase in ((mine, slot_send, slot_here, 6), (opposite, slot_far_send, slot_far, 11)):
+    def to_everyone(src, dst, phase, sems=None):
+        def sem_of(away):
+            return recv_sem.at[phase] if sems is None else sems.at[-away % n_z]
+
+        keep(src.at[me], dst.at[me], sem_of(0))
+        others(lambda to, away: send(src.at[to], dst.at[me], phase, to, mine, sem_of(away)))
+
+    for at, src, dst, phase, sems in (
+        (mine, slot_send, slot_here, 6, near_sem),
+        (opposite, slot_far_send, slot_far, 11, None),
+    ):
         cut = mix_rows[:, pl.ds(pl.multiple_of(at * quarter, quarter), quarter)].astype(BF16)
         to_slabs(
             [dot(jnp.where(before_t == float(s), named_t, 0.0).astype(BF16), cut) for s in range(CAP)], src
         )
-        to_everyone(src, dst, phase)
+        to_everyone(src, dst, phase, sems)
     mix_rows[...] = middle.astype(F32)
 
-    arrive(slot_here, recv_sem.at[6])
     sides = (1, n_tp - 1)
-    for step in sides:
-        send(slot_here, slot_all.at[mine], 7, me, tp_at(step), slot_sem.at[mine])
+    for away in (0, 1, -1, 2, -2, 3, -3, 4):
+        at, blocks = plane_of(slot_here, away)
+        arrive(blocks, near_sem.at[away % n_z])
+        for step in sides:
+            send(blocks, slot_all.at[mine, pl.ds(at, plane)], 7, me, tp_at(step), slot_sem.at[mine])
     loads[first_big + 1].wait()
     loads[first_big + 2].wait()
 
@@ -542,7 +589,10 @@
         else:
             arrive(slot_all.at[at], slot_sem.at[at])
             source = slot_all[at]
-        part = jnp.concatenate([jnp.concatenate(p, axis=1) for p in from_slabs(source)], axis=0).astype(BF16)
+        part = jnp.concatenate(
+            [jnp.concatenate(p, axis=1).reshape(n_z, 1, plane, quarter) for p in from_slabs(source)], axis=1
+        )
+        part = part.reshape(n_ep * CAP, quarter).astype(BF16)
         feats = pl.ds(pl.multiple_of(at * quarter, quarter), quarter)
         gate_part, up_part = dot(part, w_gate[feats, :]), dot(part, w_up[feats, :])
         gate = gate_part if gate is None else gate + gate_part
@@ -556,21 +606,52 @@
     def down(at):
         return dot(hidden, w_down[:, pl.ds(pl.multiple_of(at * quarter, quarter), quarter)]).astype(BF16)
 
-    def slabs_back(values, src, dst, phase):
-        to_slabs([values[s * n_ep : (s + 1) * n_ep] for s in range(CAP)], src)
-        to_everyone(src, dst, phase)
-
-    for step in sides:
+    planes = [n_z // 2 + (k + 1) // 2 * (1 if k % 2 else -1) for k in range(n_z)]
+
+    def block_of(away):
+        at = lax.rem(base + away % n_z * plane, n_ep)
+        return at, pl.ds(pl.multiple_of(at * CAP, plane * CAP), plane * CAP)
+
+    for side, step in enumerate(sides):
         at = tp_at(step)
         down_send[at] = down(at)
-        send(down_send.at[at], down_all.at[mine], 8, me, at, slot_sem.at[n_tp + mine])
-    slabs_back(down(opposite).astype(F32), back_far_send, back_far, 12)
-    total = down(mine).astype(F32)
-    for step in sides:
-        at = tp_at(step)
-        arrive(down_all.at[at], slot_sem.at[n_tp + at])
-        total += down_all[at].astype(F32)
-    slabs_back(total, back_send, back_all, 9)
+        for away in planes:
+            block = block_of(away)[1]
+            send(
+                down_send.at[at, block],
+                down_all.at[mine, block],
+                8,
+                me,
+                at,
+                down_sem.at[side * n_z + away % n_z],
+            )
+    values = down(opposite).astype(F32).reshape(n_z, CAP, plane, quarter)
+    to_slabs([values[:, s].reshape(n_ep, quarter) for s in range(CAP)], back_far_send)
+    to_everyone(back_far_send, back_far, 12)
+    down_all[mine] = down(mine)
+
+    for away in planes:
+        at, block = block_of(away)
+        total = down_all[mine, block].astype(F32)
+        for side, step in enumerate(sides):
+            source = tp_at(n_tp - step)
+            arrive(down_all.at[source, block], down_sem.at[side * n_z + away % n_z])
+            total += down_all[source, block].astype(F32)
+        for s in range(CAP):
+            for t in range(tiles):
+                wide_rows[pl.ds(at * slab + s * tiles + t, plane, stride=slab), :] = total[
+                    s * plane : (s + 1) * plane, t * LANES : (t + 1) * LANES
+                ]
+        slabs = wide_rows[pl.ds(pl.multiple_of(at * slab, plane * slab), plane * slab), :]
+        back_send[pl.ds(at, plane)] = slabs.astype(BF16).reshape(plane, slab, LANES)
+
+        def send_back(i, at=at):
+            to = at + member_at(i)
+            send(back_send.at[to], back_all.at[me], 9, to, mine)
+
+        if away % n_z == 0:
+            keep(back_send.at[me], back_all.at[me], recv_sem.at[9])
+        loop(0 if away % n_z else 1, plane, send_back)
 
     for n, (buffer, phase) in enumerate(((back_far, 12), (back_all, 9))):
         arrive(buffer, recv_sem.at[phase])
@@ -593,11 +674,13 @@
     sent(rows_all.at[pl.ds(0, plane // 2 - 1), 0], 0)
     sent(rows_all.at[:, core], 13)
     sent(moe_all.at[0, pl.ds(0, n_tp - 1)], 14)
-    sent(proj_all.at[pl.ds(0, n_ep - 1)], 1)
+    sent(pair_all.at[pl.ds(0, n_ep - 1)], 1)
+    sent(val_all.at[pl.ds(0, n_ep - 1)], 15)
     sent(out_all.at[pl.ds(0, n_z - 1)], 2)
     sent(slot_far.at[pl.ds(0, n_ep - 1)], 11)
     sent(back_far.at[pl.ds(0, n_ep - 1)], 12)
-    sent(qkv_all.at[pl.ds(0, plane - 1)], 3)
+    sent(pair_in.at[pl.ds(0, plane - 1)], 3)
+    sent(val_in.at[pl.ds(0, plane - 1)], 16)
     sent(read_all.at[pl.ds(0, plane - 1)], 4)
     sent(part_all.at[pl.ds(0, n_tp * plane - 1)], 5)
     sent(slot_here.at[pl.ds(0, n_ep - 1)], 6)
@@ -673,13 +756,17 @@
     local_shapes = [a.shape[1:] if a.ndim == 3 and n >= len(operands) - 3 else a.shape for n, a in enumerate(operands)]
     scratch = [pltpu.VMEM(shape, a.dtype) for shape, a in zip(local_shapes, operands)]
     scratch += [
-        pltpu.VMEM((plane, depth + depth // 2, 2 * HEAD_DIM), BF16),
-        pltpu.VMEM((n_ep, depth + depth // 2, 2 * HEAD_DIM), BF16),
+        pltpu.VMEM((plane, depth, 2 * HEAD_DIM), BF16),
+        pltpu.VMEM((n_ep, depth, 2 * HEAD_DIM), BF16),
+        pltpu.VMEM((plane, depth // 2, 2 * HEAD_DIM), BF16),
+        pltpu.VMEM((n_ep, depth // 2, 2 * HEAD_DIM), BF16),
         pltpu.VMEM((n_z, out_cols, quarter), BF16),
         pltpu.VMEM((plane // 2, 2, seqs, width), BF16),
         pltpu.VMEM((plane * seqs, width), BF16),
-        pltpu.VMEM((plane, seqs, WIDE), BF16),
-        pltpu.VMEM((plane, seqs, WIDE), BF16),
+        pltpu.VMEM((plane, seqs, 2 * HEAD_DIM), BF16),
+        pltpu.VMEM((plane, seqs, 2 * HEAD_DIM), BF16),
+        pltpu.VMEM((plane, seqs, 2 * HEAD_DIM), BF16),
+        pltpu.VMEM((plane, seqs, 2 * HEAD_DIM), BF16),
         pltpu.VMEM((heads * seqs, HEAD_DIM), F32),
         pltpu.VMEM((heads * seqs, HEAD_DIM), F32),
         pltpu.VMEM((2, heads, HEAD_DIM), F32),
@@ -705,10 +792,13 @@
         pltpu.VMEM((2, seqs, quarter), BF16),
         pltpu.VMEM((2, n_tp, seqs, quarter), BF16),
         pltpu.SemaphoreType.DMA((len(operands),)),
-        pltpu.SemaphoreType.DMA((15,)),
-        pltpu.SemaphoreType.DMA((15,)),
+        pltpu.SemaphoreType.DMA((17,)),
+        pltpu.SemaphoreType.DMA((17,)),
         pltpu.SemaphoreType.DMA((n_z,)),
-        pltpu.SemaphoreType.DMA((2 * n_tp,)),
+        pltpu.SemaphoreType.DMA((n_z,)),
+        pltpu.SemaphoreType.DMA((n_z,)),
+        pltpu.SemaphoreType.DMA((n_tp,)),
+        pltpu.SemaphoreType.DMA((2 * n_z,)),
     ]
     return pl.pallas_call(
         functools.partial(kernel, n_ep, n_tp),

time: 79.6 us -> 74.7 us (0.938)
  Pallas kernels: 76.9 us -> 72 us
    pallas_call x1, Pallas kernels: 76.9 us -> 72 us  [local(): pl.pallas_call(functools.partial(kernel, n_ep, n_tp), out_shape=(jax.Shap...]
where the time goes in v3:
time: 74.7 us; the launch traced here: 74.6 us
  Pallas kernels  72 us (96%)
  local copies, waits for them, and re-layouts  1.95 us (3%)
    pallas_call x1, Pallas kernels, local(): pl.pallas_call(functools.partial(kernel, n_ep, n_tp), out_shape=(jax.Shap...  72 us
    unnamed x2, local copies, waits for them, and re-layouts  1.95 us

profile of v3, /device:TPU:1, one launch (start us, length us, event | category | flops | bytes accessed | tf_op | source)
XLA Modules:
  0.0 74.6 jit_solution(17104079897969904812)
XLA Ops:
  0.6 72.0 %shard_map.230 = (bf16[16,2048]{1,0:T(8,128)(2,1)S(1)}, f32[16,8,4096]{2,1,0:T(8,128)S(1)}) custom-call(bf16[16,2048]{1,0:T(8,128)(2,1)} %layer_in_far.1, bf16[32,512]{1,0:T(8,128)(2,1)} %rec_weight_far.1, bf16[32,512]{1,0:T(8,128)(2,1)} %key_weight_far.1, bf16[32,512]{1,0:T(8,128)(2,1)} %val_weight_far.1, bf16[32,512]{1,0:T(8,128)(2,1)} %bitcast.15, ...), custom_call_target="tpu_custom_call" | custom-call | tf_op jit(solution)/shard_map/pallas_call | solution.py:803
  72.7 0.6 copy.27
  73.3 1.3 %copy.28 = f32[16,8,4096]{2,1,0:T(8,128)} copy(f32[16,8,4096]{2,1,0:T(8,128)S(1)} %get-tuple-element.5) | data formatting | bytes 4194304

commit v4 on v3

--- a/solution.py
+++ b/solution.py
@@ -210,7 +210,7 @@
     depth = rec_weight.shape[0]
     out_cols = out_send.shape[0]
 
-    for load in loads[:first_big]:
+    for load in loads[:5]:
         load.start()
 
     me = lax.axis_index("ep")
@@ -280,6 +280,8 @@
 
     loop(plane, plane * n_tp, greet_plane)
 
+    for load in loads[5:first_big]:
+        load.start()
     for load in loads[:5]:
         load.wait()
     for h in range(heads):
@@ -393,12 +395,6 @@
     sibling = me + 1 - 2 * core
     send(rows_all.at[:, core], rows_all.at[:, core], 13, sibling, mine)
     forward(val_wave)
-    keep(out_send, out_all.at[z_me], recv_sem.at[2])
-
-    def send_out(i):
-        send(out_send, out_all.at[z_me], 2, z_at(i), mine)
-
-    loop(1, n_z, send_out)
 
     arrive(rows_all.at[:, 1 - core], recv_sem.at[13])
 
@@ -407,34 +403,6 @@
         normed_all[pl.ds(pl.multiple_of(i * seqs, seqs), seqs), :] = values
 
     loop(0, plane, norm_rows)
-
-    arrive_wave(pair_wave)
-    normed = normed_all[...]
-    pair_sum = dot(normed, pair_all[...].reshape(n_ep * depth, 2 * HEAD_DIM))
-    pair_out[...] = pair_sum.astype(BF16).reshape(plane, seqs, 2 * HEAD_DIM)
-
-    def share(src, dst, phase):
-        keep(src.at[member], dst.at[member], recv_sem.at[phase])
-
-        def one(i):
-            to = member_at(i)
-            send(src.at[to], dst.at[member], phase, base + to, mine)
-
-        loop(1, plane, one)
-
-    share(pair_out, pair_in, 3)
-
-    arrive_wave(val_wave)
-    vals = val_all[...]
-    vals = jnp.concatenate([vals, vals], axis=1).reshape(n_ep * depth, 2 * HEAD_DIM)
-    spread = (n_ep * depth, 2 * HEAD_DIM)
-    first = lax.rem(iota(spread, 0), depth) < depth // 2
-    vals = jnp.where(first == (iota(spread, 1) < HEAD_DIM), vals.astype(F32), 0.0).astype(BF16)
-    val_sum = dot(normed, vals)
-    val_sum = val_sum[:, :HEAD_DIM] + val_sum[:, HEAD_DIM:]
-    val_sum = jnp.concatenate([val_sum, jnp.zeros_like(val_sum)], axis=1)
-    val_out[...] = val_sum.astype(BF16).reshape(plane, seqs, 2 * HEAD_DIM)
-    share(val_out, val_in, 16)
 
     turn = one_hot(
         iota((rows, rows), 1)
@@ -450,6 +418,40 @@
     decay = turned[:, :HEAD_DIM] + turned[:, HEAD_DIM : 2 * HEAD_DIM]
     rate = turned[:, 2 * HEAD_DIM : 3 * HEAD_DIM] + turned[:, 3 * HEAD_DIM :]
 
+    arrive_wave(pair_wave)
+    normed = normed_all[...]
+    pair_sum = dot(normed, pair_all[...].reshape(n_ep * depth, 2 * HEAD_DIM))
+    pair_out[...] = pair_sum.astype(BF16).reshape(plane, seqs, 2 * HEAD_DIM)
+
+    def share(src, dst, phase):
+        keep(src.at[member], dst.at[member], recv_sem.at[phase])
+
+        def one(i):
+            to = member_at(i)
+            send(src.at[to], dst.at[member], phase, base + to, mine)
+
+        loop(1, plane, one)
+
+    share(pair_out, pair_in, 3)
+    keep(out_send, out_all.at[z_me], recv_sem.at[2])
+
+    def send_out(i):
+        send(out_send, out_all.at[z_me], 2, z_at(i), mine)
+
+    loop(1, n_z, send_out)
+
+    arrive_wave(val_wave)
+    vals = val_all[...]
+    vals = jnp.concatenate([vals, vals], axis=1).reshape(n_ep * depth, 2 * HEAD_DIM)
+    spread = (n_ep * depth, 2 * HEAD_DIM)
+    first = lax.rem(iota(spread, 0), depth) < depth // 2
+    vals = jnp.where(first == (iota(spread, 1) < HEAD_DIM), vals.astype(F32), 0.0).astype(BF16)
+    val_sum = dot(normed, vals)
+    val_sum = val_sum[:, :HEAD_DIM] + val_sum[:, HEAD_DIM:]
+    val_sum = jnp.concatenate([val_sum, jnp.zeros_like(val_sum)], axis=1)
+    val_out[...] = val_sum.astype(BF16).reshape(plane, seqs, 2 * HEAD_DIM)
+    share(val_out, val_in, 16)
+
     arrive(pair_in, recv_sem.at[3])
     pair = dot(turn, pair_in[...].reshape(rows, 2 * HEAD_DIM))
     rec = pair[:, :HEAD_DIM]
@@ -517,11 +519,13 @@
     part_send[...] = part.astype(BF16).reshape(plane, seqs, n_z * out_cols)
     keep(part_send.at[member], part_all.at[mine * plane + member], recv_sem.at[5])
 
-    def send_part(i):
-        to = member_at(lax.rem(i, plane))
-        send(part_send.at[to], part_all.at[mine * plane + member], 5, base + to, tp_at(i // plane))
-
-    loop(1, plane * n_tp, send_part)
+    def send_part(i, step):
+        to = member_at(i)
+        send(part_send.at[to], part_all.at[mine * plane + member], 5, base + to, tp_at(step))
+
+    for step in (2, 1, n_tp - 1):
+        loop(plane // 2, plane + plane // 2, functools.partial(send_part, step=step))
+    loop(1, plane, functools.partial(send_part, step=0))
 
     arrive(part_all, recv_sem.at[5])
     for g in range(plane):

time: 74.7 us -> 72.7 us (0.973)
  Pallas kernels: 72 us -> 70 us
    pallas_call x1, Pallas kernels: 72 us -> 70 us  [local(): pl.pallas_call(functools.partial(kernel, n_ep, n_tp), out_shape=(jax.Shap...]
where the time goes in v4:
time: 72.7 us; the launch traced here: 72.6 us
  Pallas kernels  70 us (96%)
  local copies, waits for them, and re-layouts  1.95 us (3%)
    pallas_call x1, Pallas kernels, local(): pl.pallas_call(functools.partial(kernel, n_ep, n_tp), out_shape=(jax.Shap...  70 us
    unnamed x2, local copies, waits for them, and re-layouts  1.95 us

profile of v4, /device:TPU:1, one launch (start us, length us, event | category | flops | bytes accessed | tf_op | source)
XLA Modules:
  0.0 72.6 jit_solution(8196738445339930868)
XLA Ops:
  0.6 70.0 %shard_map.230 = (bf16[16,2048]{1,0:T(8,128)(2,1)S(1)}, f32[16,8,4096]{2,1,0:T(8,128)S(1)}) custom-call(bf16[16,2048]{1,0:T(8,128)(2,1)} %layer_in_far.1, bf16[32,512]{1,0:T(8,128)(2,1)} %rec_weight_far.1, bf16[32,512]{1,0:T(8,128)(2,1)} %key_weight_far.1, bf16[32,512]{1,0:T(8,128)(2,1)} %val_weight_far.1, bf16[32,512]{1,0:T(8,128)(2,1)} %bitcast.15, ...), custom_call_target="tpu_custom_call" | custom-call | tf_op jit(solution)/shard_map/pallas_call | solution.py:807
  70.7 0.6 copy.27
  71.3 1.3 %copy.28 = f32[16,8,4096]{2,1,0:T(8,128)} copy(f32[16,8,4096]{2,1,0:T(8,128)S(1)} %get-tuple-element.5) | data formatting | bytes 4194304
